TPU v7x, 128 devices: a whole 4x4x4 slice. The times are simulated.
128 devices in a mesh: ep: 128 (over z, y, x, core).
Axes of the slice: x: 4, y: 4, z: 4, core: 2. Of those that a mesh axis runs over, the one named last changes fastest.
Arguments:
- tokens: bfloat16 [2048, 1024], P('ep'), may hold values from -6 to 6
- lengths: int32 [2048], P('ep'), may hold values from 1 to 8191
- cache_keys: bfloat16 [2048, 128, 512], P('ep'), may hold values from -6 to 6
- cache_values: bfloat16 [2048, 128, 1024], P('ep'), may hold values from -6 to 6
- retention_state: float32 [2048, 4, 128, 256], P('ep'), may hold values from -24 to 24
- mix_gain: float32 [1024], replicated, may hold values from 0.1 to 1.9
- query_weight: bfloat16 [1024, 512], replicated, may hold values from -0.1875 to 0.1875
- key_weight: bfloat16 [1024, 512], replicated, may hold values from -0.1875 to 0.1875
- value_weight: bfloat16 [1024, 1024], replicated, may hold values from -0.1875 to 0.1875
- out_weight: bfloat16 [1024, 1024], replicated, may hold values from -0.1875 to 0.1875
- ffn_gain: float32 [1024], replicated, may hold values from 0.1 to 1.9
- routes: int32 [2048, 6], P('ep'), may hold values from 0 to 127, all different within a row; in each aligned block of 16 rows (0 to 15, 16 to 31, ...) at most 2 rows name the same one
- route_scores: float32 [2048, 6], P('ep'), may hold values from 0.05 to 1
- expert_gate: bfloat16 [128, 1024, 256], P('ep'), may hold values from -0.1875 to 0.1875
- expert_up: bfloat16 [128, 1024, 256], P('ep'), may hold values from -0.1875 to 0.1875
- expert_down: bfloat16 [128, 256, 1024], P('ep'), may hold values from -0.375 to 0.375
- shared_gate: bfloat16 [1024, 256], replicated, may hold values from -0.1875 to 0.1875
- shared_up: bfloat16 [1024, 256], replicated, may hold values from -0.1875 to 0.1875
- shared_down: bfloat16 [256, 1024], replicated, may hold values from -0.375 to 0.375
- dense_gate: bfloat16 [4096, 1024], P('ep'), may hold values from -0.1875 to 0.1875
- dense_up: bfloat16 [4096, 1024], P('ep'), may hold values from -0.1875 to 0.1875
- dense_down: bfloat16 [4096, 1024], P('ep'), may hold values from -0.09375 to 0.09375
- dense_mix: float32 [1024], replicated, may hold values from -3 to 3
Outputs:
- layer_out: bfloat16 [2048, 1024], P('ep')
- new_keys: bfloat16 [2048, 512], P('ep')
- new_values: bfloat16 [2048, 1024], P('ep')
Inputs may be any that keep to these rules, and one draw needn't show every extreme that they name: `routes`: each row names 6 different experts; among the rows of one device no expert is named more than 2 times.
All inputs are finite; a program needn't handle non-finite values.
Results may differ from a plain program's by a relative error of at most 0.012.
Values may be sent and summed in bfloat16 or wider, within the bound.
A program may use at most 128 MiB of HBM per device.

v0:
```python
import jax
import jax.numpy as jnp
from jax import lax
from jax.sharding import PartitionSpec as P

eps = 1e-06
route_scale = 2.5
rope_base = 10000.0


def side_by_side(arrays, axis, dim, along):
    ends, at = ([], 0)
    for a in arrays[:-1]:
        at += a.shape[along]
        ends.append(at)
    both = jnp.concatenate(arrays, axis=along)
    return tuple(jnp.split(lax.all_gather(both, axis, axis=dim, tiled=True), ends, axis=along))


def normed(values):
    return values * lax.rsqrt(jnp.mean(values * values, axis=-1, keepdims=True) + eps)


def log_decay(head_count):
    return jnp.log1p(-jnp.exp2(-5.0 - jnp.arange(head_count, dtype=jnp.float32)))


def rotate(values, positions):
    half_size = values.shape[-1] // 2
    inverse = rope_base ** (-jnp.arange(half_size, dtype=jnp.float32) / half_size)
    angles = positions.astype(jnp.float32)[:, None, None] * inverse[None, None, :]
    cosine = jnp.cos(angles)
    sine_part = jnp.sin(angles)
    first_half = values[..., :half_size]
    second = values[..., half_size:]
    return jnp.concatenate(
        [first_half * cosine - second * sine_part, first_half * sine_part + second * cosine],
        axis=-1,
    )


def swiglu(inputs, w_gate, w_up, w_down):
    gate_part = jnp.dot(inputs, w_gate, preferred_element_type=jnp.float32)
    up_part = jnp.dot(inputs, w_up, preferred_element_type=jnp.float32)
    hidden = (jax.nn.silu(gate_part) * up_part).astype(jnp.bfloat16)
    return jnp.dot(hidden, w_down, preferred_element_type=jnp.float32)


def dense_part(inputs, gate_rows, up_rows, down_rows):
    contract = (((1,), (1,)), ((), ()))
    gate_part = lax.dot_general(inputs, gate_rows, contract, preferred_element_type=jnp.float32)
    up_part = lax.dot_general(inputs, up_rows, contract, preferred_element_type=jnp.float32)
    hidden = (jax.nn.silu(gate_part) * up_part).astype(jnp.bfloat16)
    return jnp.dot(hidden, down_rows, preferred_element_type=jnp.float32)


def retain(
    tokens, lengths, mix_gain, w_query, w_key, w_value, w_out, cache_keys, cache_values, carry_state
):
    seq_count, head_count, key_size, value_size = carry_state.shape
    block_size = cache_keys.shape[1]
    widened = tokens.astype(jnp.float32)
    normal_in = (normed(widened) * mix_gain).astype(jnp.bfloat16)
    raw_query = jnp.dot(normal_in, w_query, preferred_element_type=jnp.float32).reshape(
        seq_count, head_count, key_size
    )
    raw_key = jnp.dot(normal_in, w_key, preferred_element_type=jnp.float32).reshape(
        seq_count, head_count, key_size
    )
    raw_value = jnp.dot(normal_in, w_value, preferred_element_type=jnp.float32).reshape(
        seq_count, head_count, value_size
    )
    queries = (rotate(raw_query, lengths) * key_size ** (-0.5)).astype(jnp.bfloat16)
    new_keys = rotate(raw_key, lengths).astype(jnp.bfloat16)
    new_values = raw_value.astype(jnp.bfloat16)
    filled = lengths % block_size
    decay_rate = log_decay(head_count)
    places = jnp.arange(block_size, dtype=jnp.int32)
    stored_keys = cache_keys.reshape(seq_count, block_size, head_count, key_size)
    stored_values = cache_values.reshape(seq_count, block_size, head_count, value_size)
    scores = jnp.einsum("shd,sjhd->shj", queries, stored_keys, preferred_element_type=jnp.float32)
    distance = jnp.maximum(filled[:, None] - places[None, :], 0).astype(jnp.float32)
    live_mask = places[None, :] < filled[:, None]
    weighted = jnp.where(
        live_mask[:, None, :],
        scores * jnp.exp(distance[:, None, :] * decay_rate[None, :, None]),
        0.0,
    ).astype(jnp.bfloat16)
    own_weight = jnp.sum(
        queries.astype(jnp.float32) * new_keys.astype(jnp.float32), axis=-1
    ).astype(jnp.bfloat16)
    inside = jnp.einsum(
        "shj,sjhe->she", weighted, stored_values, preferred_element_type=jnp.float32
    )
    inside = inside + own_weight.astype(jnp.float32)[:, :, None] * new_values.astype(jnp.float32)
    carried = jnp.einsum("shd,shde->she", queries.astype(jnp.float32), carry_state)
    carried = (
        carried
        * jnp.exp((filled.astype(jnp.float32)[:, None] + 1.0) * decay_rate[None, :])[:, :, None]
    )
    headed = (
        normed(inside + carried).astype(jnp.bfloat16).reshape(seq_count, head_count * value_size)
    )
    mixer_out = jnp.dot(headed, w_out, preferred_element_type=jnp.float32)
    residual = widened + normed(mixer_out)
    return (
        residual,
        new_keys.reshape(seq_count, head_count * key_size),
        new_values.reshape(seq_count, head_count * value_size),
    )


def capacity(seq_count, top_count, expert_count):
    return max(2, seq_count * top_count * 8 // (3 * expert_count))


def exchanged_experts(normal_ffn, routes, route_weight, expert_gate, expert_up, expert_down):
    seq_count, top_count = routes.shape
    model_width = normal_ffn.shape[1]
    expert_count = lax.axis_size("ep") * expert_gate.shape[0]
    slot_count = capacity(seq_count, top_count, expert_count)
    flat_routes = routes.reshape(-1)
    onehot = (flat_routes[:, None] == jnp.arange(expert_count, dtype=jnp.int32)[None, :]).astype(
        jnp.int32
    )
    slot_ids = jnp.sum((jnp.cumsum(onehot, axis=0) - 1) * onehot, axis=1)
    target = flat_routes * slot_count + slot_ids
    placed = (
        target[None, :] == jnp.arange(expert_count * slot_count, dtype=jnp.int32)[:, None]
    ).astype(jnp.float32)
    chosen = jnp.sum(placed.reshape(expert_count * slot_count, seq_count, top_count), axis=2)
    outgoing = jnp.dot(
        chosen.astype(jnp.bfloat16), normal_ffn, preferred_element_type=jnp.float32
    ).astype(jnp.bfloat16)
    outgoing = outgoing.reshape(expert_count, slot_count, model_width)
    arrived = lax.all_to_all(outgoing, "ep", split_axis=0, concat_axis=0, tiled=True)
    outputs = swiglu(
        arrived.reshape(-1, model_width), expert_gate[0], expert_up[0], expert_down[0]
    ).astype(jnp.bfloat16)
    returned = lax.all_to_all(
        outputs.reshape(arrived.shape), "ep", split_axis=0, concat_axis=0, tiled=True
    )
    weights_by_slot = placed * route_weight.reshape(-1)[None, :]
    combine = jnp.sum(
        weights_by_slot.reshape(expert_count * slot_count, seq_count, top_count), axis=2
    )
    return lax.dot_general(
        combine, returned.reshape(-1, model_width).astype(jnp.float32), (((0,), (0,)), ((), ()))
    )


def per_device(
    tokens,
    lengths,
    cache_keys,
    cache_values,
    retention_state,
    mix_gain,
    query_weight,
    key_weight,
    value_weight,
    out_weight,
    ffn_gain,
    routes,
    route_scores,
    expert_gate,
    expert_up,
    expert_down,
    shared_gate,
    shared_up,
    shared_down,
    dense_gate,
    dense_up,
    dense_down,
    dense_mix,
):
    residual, new_keys, new_values = retain(
        tokens,
        lengths,
        mix_gain,
        query_weight,
        key_weight,
        value_weight,
        out_weight,
        cache_keys,
        cache_values,
        retention_state,
    )
    normal_ffn = (normed(residual) * ffn_gain).astype(jnp.bfloat16)
    shared_out = swiglu(normal_ffn, shared_gate, shared_up, shared_down)
    gated = jax.nn.sigmoid(dense_mix)
    route_weight = route_scores / jnp.sum(route_scores, axis=-1, keepdims=True) * route_scale
    pieces = side_by_side((dense_gate, dense_up, dense_down), "ep", 0, 1)
    dense_out = dense_part(normal_ffn, pieces[0], pieces[1], pieces[2])
    combined = (
        shared_out
        + gated * dense_out
        + exchanged_experts(normal_ffn, routes, route_weight, expert_gate, expert_up, expert_down)
    )
    layer_out = (residual + normed(combined)).astype(jnp.bfloat16)
    return (layer_out, new_keys, new_values)


def solution(mesh):
    in_specs = (
        P("ep", None),
        P("ep"),
        P("ep", None, None),
        P("ep", None, None),
        P("ep", None, None, None),
        P(),
        P(),
        P(),
        P(),
        P(),
        P(),
        P("ep", None),
        P("ep", None),
        P("ep", None, None),
        P("ep", None, None),
        P("ep", None, None),
        P(),
        P(),
        P(),
        P("ep", None),
        P("ep", None),
        P("ep", None),
        P(),
    )
    out_specs = (P("ep", None), P("ep", None), P("ep", None))
    return jax.shard_map(
        per_device, mesh=mesh, in_specs=in_specs, out_specs=out_specs, check_vma=False
    )
```

profile of v0, /device:TPU:1, one launch (start us, length us, event | category | flops | bytes accessed | tf_op | source)
XLA Modules:
  0.0 143.6 jit_solution(467105404568314871)
XLA Ops:
  7.2 1.7 %pad_maximum_fusion = bf16[32,3072]{1,0:T(8,128)(2,1)} fusion(bf16[32,1024]{1,0:T(8,128)(2,1)} %param.44, bf16[32,1024]{1,0:T(8,128)(2,1)} %param.43, bf16[32,1024]{1,0:T(8,128)(2,1)} %param.42), kind=kLoop, calls=%fused_computation.35 | loop fusion | flops 589824 | bytes 393216 | tf_op jit(solution)/shard_map/concatenate | solution.py:16
  9.0 0.9 fusion.41
  9.9 1.6 %fusion.67 = f32[16,512]{1,0:T(8,128)S(1)} fusion(bf16[1024,512]{1,0:T(8,128)(2,1)} %param.29, bf16[16,1024]{1,0:T(8,128)(2,1)} %param.23, f32[1024]{0:T(1024)} %param.28, f32[16]{0:T(128)S(1)} %add_rsqrt_fusion.4), kind=kOutput, calls=%fused_computation.108 | convolution fusion | flops 16842752 | bytes 1118272 | tf_op jit(solution)/shard_map/dot_general | solution.py:64
  12.2 1.5 %fusion.65 = f32[16,512]{1,0:T(8,128)S(1)} fusion(bf16[1024,512]{1,0:T(8,128)(2,1)} %param.30, bf16[16,1024]{1,0:T(8,128)(2,1)} %param.23, f32[1024]{0:T(1024)} %param.28, f32[16]{0:T(128)S(1)} %add_rsqrt_fusion.4), kind=kOutput, calls=%fused_computation.107 | convolution fusion | flops 16842752 | bytes 1118272 | tf_op jit(solution)/shard_map/dot_general | solution.py:67
  13.8 3.9 %copy.44 = bf16[16,128,512]{1,2,0:T(8,128)(2,1)} copy(bf16[16,128,512]{2,1,0:T(8,128)(2,1)} %param.25) | data formatting | bytes 4194304 | tf_op jit(solution)/shard_map/reshape | solution.py:79
  18.2 2.0 %convolution_convert_fusion.2 = bf16[16,1024]{1,0:T(8,128)(2,1)S(1)} fusion(bf16[1024,1024]{1,0:T(8,128)(2,1)} %param.31, bf16[16,1024]{1,0:T(8,128)(2,1)S(1)} %copy-done.1, f32[1024]{0:T(1024)S(1)} %copy-done.4, f32[16]{0:T(128)S(1)} %add_rsqrt_fusion.4), kind=kOutput, calls=%fused_computation.18 | convolution fusion | flops 33636352 | bytes 2166848 | tf_op jit(solution)/shard_map/dot_general | solution.py:70
  20.5 2.2 %fusion.50 = f32[16,4,1,128]{3,2,1,0:T(1,128)S(1)} fusion(bf16[16,128,4,128]{1,3,2,0:T(8,128)(2,1)} %bitcast.56, bf16[16,4,128,1]{2,1,0,3:T(4,128)(2,1)S(1)} %bitcast.58), kind=kOutput, calls=%fused_computation.72 | convolution fusion | flops 2097152 | bytes 2146304 | tf_op jit(solution)/shard_map/shd,sjhd->shj/dot_general | solution.py:81
  22.9 2.9 %fusion.12 = f32[16,4,1,256]{3,2,1,0:T(1,128)S(1)} fusion(bf16[16,16,4,8,256]{4,3,2,1,0:T(8,128)(2,1)} %bitcast.57, bf16[16,4,128,1]{2,1,0,3:T(4,128)(2,1)S(1)} %fusion.52), kind=kOutput, calls=%fused_computation.8 | convolution fusion | flops 4194304 | bytes 4276224 | tf_op jit(solution)/shard_map/shj,sjhe->she/dot_general | solution.py:92
  25.8 4.1 %fusion.48 = f32[16,4,1,256]{3,2,1,0:T(1,128)S(1)} fusion(f32[16,4,128,256]{3,2,1,0:T(8,128)} %param.27, bf16[16,4,128,1]{2,1,0,3:T(4,128)(2,1)S(1)} %bitcast.59), kind=kOutput, calls=%fused_computation.70 | convolution fusion | flops 4194304 | bytes 8470528 | tf_op jit(solution)/shard_map/shd,shde->she/dot_general | solution.py:96
  33.1 29.4 %all_to_all.10 = bf16[128,2,1024]{2,1,0:T(2,128)(2,1)} all-to-all(bf16[128,2,1024]{2,1,0:T(2,128)(2,1)S(1)} %reshape.268), channel_id=1, replica_groups=mesh['ep'=128] {'ep'}, dimensions={0} | all-to-all | bytes 1048576 | tf_op jit(solution)/shard_map/all_to_all | solution.py:136
  62.5 1.2 reshape.269
  63.7 1.3 fusion.27
  65.1 1.9 %convolution_convert_fusion = bf16[256,1024]{1,0:T(8,128)(2,1)S(1)} fusion(bf16[256,1024]{1,0:T(8,128)(2,1)S(1)} %reshape.269, bf16[1,256,1024]{2,1,0:T(8,128)(2,1)} %param.38, bf16[1,1024,256]{2,1,0:T(8,128)(2,1)} %param.37, f32[256,256]{1,0:T(8,128)S(1)} %fusion.27), kind=kOutput, calls=%fused_computation.11 | convolution fusion | flops 269090816 | bytes 2359296 | tf_op jit(solution)/shard_map/dot_general | solution.py:46
  67.0 1.0 reshape.270
  68.1 5.6 %all-to-all-start.1 = ((bf16[128,2,1024]{2,1,0:T(2,128)(2,1)}), bf16[128,2,1024]{2,1,0:T(2,128)(2,1)S(1)}, u32[]{:S(2)}, u32[]{:S(2)}) async-start(bf16[128,2,1024]{2,1,0:T(2,128)(2,1)} %reshape.270), calls=%async_computation.1 | async-start | bytes 1048576 | tf_op jit(solution)/shard_map/all_to_all | solution.py:140
  74.3 1.3 add_divide_fusion
  75.6 1.2 fusion.71
  76.8 16.5 %all-to-all-done.1 = bf16[128,2,1024]{2,1,0:T(2,128)(2,1)S(1)} async-done(((bf16[128,2,1024]{2,1,0:T(2,128)(2,1)}), bf16[128,2,1024]{2,1,0:T(2,128)(2,1)S(1)}, u32[]{:S(2)}, u32[]{:S(2)}) %all-to-all-start.1) | async-done | bytes 524320 | tf_op jit(solution)/shard_map/all_to_all | solution.py:140
  93.5 23.9 %all-gather.2.cloned.1.call-done = bf16[4096,3072]{1,0:T(8,128)(2,1)} async-done(((bf16[32,3072]{1,0:T(8,128)(2,1)}), bf16[4096,3072]{1,0:T(8,128)(2,1)}) %all-gather.2.cloned.1.call-update) | async-done | bytes 25165840 | tf_op jit(solution)/shard_map/all_gather | solution.py:17
  117.4 5.7 %fusion.4 = f32[16,4096]{1,0:T(8,128)S(1)} fusion(bf16[16,1024]{1,0:T(8,128)(2,1)S(1)} %multiply_convert_fusion, bf16[4096,3072]{1,0:T(8,128)(2,1)} %all-gather.2.cloned.1.call-done), kind=kOutput, calls=%fused_computation.4 | convolution fusion | flops 134217728 | bytes 8683520 | tf_op jit(solution)/shard_map/dot_general | solution.py:51
  123.1 9.9 %fusion.18 = f32[16,1024]{1,0:T(8,128)} fusion(bf16[4096,3072]{1,0:T(8,128)(2,1)} %all-gather.2.cloned.1.call-done, bf16[16,1024]{1,0:T(8,128)(2,1)S(1)} %multiply_convert_fusion, f32[16,4096]{1,0:T(8,128)S(1)} %fusion.4, f32[1024]{0:T(1024)} %add_divide_fusion), kind=kOutput, calls=%fused_computation.17 | convolution fusion | flops 268845056 | bytes 17141760 | tf_op jit(solution)/shard_map/dot_general | solution.py:54
  132.9 1.5 %convolution_add_fusion.1 = f32[16,1024]{1,0:T(8,128)S(1)} fusion(f32[16,1024]{1,0:T(8,128)} %fusion.18, bf16[256,1024]{1,0:T(8,128)(2,1)S(1)} %copy-done.2, bf16[16,1024]{1,0:T(8,128)(2,1)S(1)} %multiply_convert_fusion, bf16[1024,256]{1,0:T(8,128)(2,1)} %param.40, f32[16,256]{1,0:T(8,128)S(1)} %fusion.71), kind=kOutput, calls=%fused_computation.16 | convolution fusion | flops 16818176 | bytes 1228800 | tf_op jit(solution)/shard_map/dot_general | solution.py:46
  134.4 1.0 multiply_reduce_fusion
  135.4 1.3 add_convert_fusion
  (64 shorter events, 5.6 us)
Async XLA Ops:
  7.2 24.6 %copy-start = (bf16[1024,1024]{1,0:T(8,128)(2,1)S(1)}, bf16[1024,1024]{1,0:T(8,128)(2,1)}, u32[]{:S(2)}) copy-start(bf16[1024,1024]{1,0:T(8,128)(2,1)} %param.32) | copy-start | bytes 6291460
  7.2 11.0 %copy-start.1 = (bf16[16,1024]{1,0:T(8,128)(2,1)S(1)}, bf16[16,1024]{1,0:T(8,128)(2,1)}, u32[]{:S(2)}) copy-start(bf16[16,1024]{1,0:T(8,128)(2,1)} %param.23) | copy-start | bytes 98308
  7.2 11.0 %copy-start.4 = (f32[1024]{0:T(1024)S(1)}, f32[1024]{0:T(1024)}, u32[]{:S(2)}) copy-start(f32[1024]{0:T(1024)} %param.28) | copy-start | bytes 12292
  7.2 110.2 %all-gather.2.cloned.1.call-start = ((), (), s32[]{:S(2)}) async-start(), calls=%async_computation.2 | async-start | bytes 25362432 | tf_op jit(solution)/shard_map/all_gather | solution.py:17
  11.5 8.9 %copy-start.9 = (s32[16]{0:T(128)S(1)}, s32[16]{0:T(128)}, u32[]{:S(2)}) copy-start(s32[16]{0:T(128)} %param.24) | copy-start | bytes 196
  20.2 2.7 %copy-start.3 = (bf16[16,1024]{1,0:T(8,128)(2,1)}, bf16[16,1024]{1,0:T(8,128)(2,1)S(1)}, u32[]{:S(2)}) copy-start(bf16[16,1024]{1,0:T(8,128)(2,1)S(1)} %convolution_convert_fusion.2) | copy-start | bytes 98308
  25.8 4.4 %copy-start.5 = (s32[16,6]{0,1:T(8,128)S(1)}, s32[16,6]{0,1:T(8,128)}, u32[]{:S(2)}) copy-start(s32[16,6]{0,1:T(8,128)} %param.34) | copy-start | bytes 1156
  25.8 5.1 %copy-start.6 = (f32[16,6]{0,1:T(8,128)S(1)}, f32[16,6]{0,1:T(8,128)}, u32[]{:S(2)}) copy-start(f32[16,6]{0,1:T(8,128)} %param.35) | copy-start | bytes 1156
  25.8 6.6 %copy-start.8 = (f32[1024]{0:T(1024)S(1)}, f32[1024]{0:T(1024)}, u32[]{:S(2)}) copy-start(f32[1024]{0:T(1024)} %param.33) | copy-start | bytes 12292
  32.2 30.3 %copy-start.7 = (f32[16]{0:T(128)}, f32[16]{0:T(128)S(1)}, u32[]{:S(2)}) copy-start(f32[16]{0:T(128)S(1)} %add_rsqrt_fusion.3) | copy-start | bytes 196
  68.1 25.2 %all-to-all-start.1 = ((bf16[128,2,1024]{2,1,0:T(2,128)(2,1)}), bf16[128,2,1024]{2,1,0:T(2,128)(2,1)S(1)}, u32[]{:S(2)}, u32[]{:S(2)}) async-start(bf16[128,2,1024]{2,1,0:T(2,128)(2,1)} %reshape.270), calls=%async_computation.1 | async-start | bytes 1048576 | tf_op jit(solution)/shard_map/all_to_all | solution.py:140
  123.1 9.9 %copy-start.2 = (bf16[256,1024]{1,0:T(8,128)(2,1)S(1)}, bf16[256,1024]{1,0:T(8,128)(2,1)}, u32[]{:S(2)}) copy-start(bf16[256,1024]{1,0:T(8,128)(2,1)} %param.41) | copy-start | bytes 1572868
Sparse Core Ops, SparseCore 0:
  11.1 106.2 all-gather.1
where the time goes:
time: 144 us
  waiting for transfers between devices  40.4 us (28%)
  matrix products  37.7 us (26%)
  blocking collectives  29.4 us (20%)
  between operations  14.3 us (10%)
  other arithmetic  8.52 us (6%)
  local copies, waits for them, and re-layouts  7.67 us (5%)
  starting transfers between devices  5.61 us (4%)
    all_to_all x1, blocking collectives, exchanged_experts(): lax.all_to_all(outgoing, 'ep', split_axis=0, concat_axis=0, tiled=True)  29.4 us
    all_gather x1, waiting for transfers between devices, side_by_side(): lax.all_gather(both, axis, axis=dim, tiled=True)  23.9 us
    all_to_all x1, waiting for transfers between devices, exchanged_experts(): lax.all_to_all(outputs.reshape(arrived.shape), 'ep', split_axis=0, concat...  16.5 us
    dot_general x1, matrix products, dense_part(): return jnp.dot(hidden, down_rows, preferred_element_type=jnp.float32)  9.86 us
    dot_general x1, matrix products, dense_part(): lax.dot_general(inputs, gate_rows, contract, preferred_element_type=jnp.f...  5.65 us
    all_to_all x1, starting transfers between devices, exchanged_experts(): lax.all_to_all(outputs.reshape(arrived.shape), 'ep', split_axis=0, concat...  5.58 us
    dot_general x1, matrix products, retain(): jnp.einsum('shd,shde->she', queries.astype(jnp.float32), carry_state)  4.06 us
    reshape x1, local copies, waits for them, and re-layouts, retain(): cache_keys.reshape(seq_count, block_size, head_count, key_size)  3.91 us
  transfers between devices with their start and end apart: 2, of which 2 were waited for; matrix products, arithmetic and copies ran while one was open for 23% of the time, Pallas kernels for 0%

commit v1 on v0

v1 whole, which is shorter than its diff:
```python
import jax
import jax.numpy as jnp
from jax import lax
from jax.experimental import pallas as pl
from jax.experimental.pallas import tpu as pltpu
from jax.sharding import PartitionSpec as P

eps = 1e-06
route_scale = 2.5
rope_base = 10000.0
MESH = pl.DeviceIdType.MESH
BF = jnp.bfloat16
F32 = jnp.float32


def normed(values):
    return values * lax.rsqrt(jnp.mean(values * values, axis=-1, keepdims=True) + eps)


def log_decay(head_count):
    return jnp.log1p(-jnp.exp2(-5.0 - jnp.arange(head_count, dtype=jnp.float32)))


def rotate(values, positions):
    half_size = values.shape[-1] // 2
    inverse = rope_base ** (-jnp.arange(half_size, dtype=jnp.float32) / half_size)
    angles = positions.astype(jnp.float32)[:, None, None] * inverse[None, None, :]
    cosine = jnp.cos(angles)
    sine_part = jnp.sin(angles)
    first_half = values[..., :half_size]
    second = values[..., half_size:]
    return jnp.concatenate(
        [first_half * cosine - second * sine_part, first_half * sine_part + second * cosine],
        axis=-1,
    )


def retain(
    tokens, lengths, mix_gain, w_query, w_key, w_value, w_out, cache_keys, cache_values, carry_state
):
    seq_count, head_count, key_size, value_size = carry_state.shape
    block_size = cache_keys.shape[1]
    widened = tokens.astype(jnp.float32)
    normal_in = (normed(widened) * mix_gain).astype(jnp.bfloat16)
    raw_query = jnp.dot(normal_in, w_query, preferred_element_type=jnp.float32).reshape(
        seq_count, head_count, key_size
    )
    raw_key = jnp.dot(normal_in, w_key, preferred_element_type=jnp.float32).reshape(
        seq_count, head_count, key_size
    )
    raw_value = jnp.dot(normal_in, w_value, preferred_element_type=jnp.float32).reshape(
        seq_count, head_count, value_size
    )
    queries = (rotate(raw_query, lengths) * key_size ** (-0.5)).astype(jnp.bfloat16)
    new_keys = rotate(raw_key, lengths).astype(jnp.bfloat16)
    new_values = raw_value.astype(jnp.bfloat16)
    filled = lengths % block_size
    decay_rate = log_decay(head_count)
    places = jnp.arange(block_size, dtype=jnp.int32)
    stored_keys = cache_keys.reshape(seq_count, block_size, head_count, key_size)
    stored_values = cache_values.reshape(seq_count, block_size, head_count, value_size)
    scores = jnp.einsum("shd,sjhd->shj", queries, stored_keys, preferred_element_type=jnp.float32)
    distance = jnp.maximum(filled[:, None] - places[None, :], 0).astype(jnp.float32)
    live_mask = places[None, :] < filled[:, None]
    weighted = jnp.where(
        live_mask[:, None, :],
        scores * jnp.exp(distance[:, None, :] * decay_rate[None, :, None]),
        0.0,
    ).astype(jnp.bfloat16)
    own_weight = jnp.sum(
        queries.astype(jnp.float32) * new_keys.astype(jnp.float32), axis=-1
    ).astype(jnp.bfloat16)
    inside = jnp.einsum(
        "shj,sjhe->she", weighted, stored_values, preferred_element_type=jnp.float32
    )
    inside = inside + own_weight.astype(jnp.float32)[:, :, None] * new_values.astype(jnp.float32)
    carried = jnp.einsum("shd,shde->she", queries.astype(jnp.float32), carry_state)
    carried = (
        carried
        * jnp.exp((filled.astype(jnp.float32)[:, None] + 1.0) * decay_rate[None, :])[:, :, None]
    )
    headed = (
        normed(inside + carried).astype(jnp.bfloat16).reshape(seq_count, head_count * value_size)
    )
    mixer_out = jnp.dot(headed, w_out, preferred_element_type=jnp.float32)
    residual = widened + normed(mixer_out)
    return (
        residual,
        new_keys.reshape(seq_count, head_count * key_size),
        new_values.reshape(seq_count, head_count * value_size),
    )


def dot(a, b):
    return jnp.dot(a, b, preferred_element_type=F32)


def dot_t(a, b):
    return lax.dot_general(a, b, (((1,), (1,)), ((), ())), preferred_element_type=F32)


def silu(v):
    return v / (1.0 + jnp.exp(-v))


def iota(shape, dim):
    return lax.broadcasted_iota(jnp.int32, shape, dim)


def ffn_kernel(
    x_ref, res_ref, routes_ref, scores_ref, mix_ref,
    eg_hbm, eu_hbm, ed_hbm, sg_hbm, su_hbm, sd_hbm, dg_hbm, du_hbm, dd_hbm,
    out_ref,
    xg, wg, dw, sbuf, rbuf, ybuf, bbuf, pbuf, qbuf,
    eg, eu, ed, sg, su, sd,
    loc, lw, w_s, w_r, d_s, d_r, x_s, x_r, a_s, a_r, b_s, b_r, p_s, p_r,
):
    me = lax.axis_index("ep")
    q = lax.rem(me, 8)
    p = lax.div(me, 8)
    z = lax.div(p, 4)
    y = lax.rem(p, 4)
    base = me - q

    def mate(k):
        return lax.rem(q + k, 8)

    def plane(dz, dy):
        return lax.rem(z + dz, 4), lax.rem(y + dy, 4)

    def device(zz, yy):
        return (zz * 4 + yy) * 8 + q

    def remote(src, dst, s, r, dev):
        return pltpu.make_async_remote_copy(
            src_ref=src, dst_ref=dst, send_sem=s, recv_sem=r, device_id=(dev,), device_id_type=MESH
        )

    barrier = pltpu.get_barrier_semaphore()
    for k in range(1, 8):
        pl.semaphore_signal(barrier, inc=1, device_id=(base + mate(k),), device_id_type=MESH)
    offsets = [(dz, dy) for dz in (0, 1, 3, 2) for dy in (0, 1, 3, 2) if (dz, dy) != (0, 0)]
    for dz, dy in offsets:
        pl.semaphore_signal(barrier, inc=1, device_id=(device(*plane(dz, dy)),), device_id_type=MESH)

    own = []
    for i, hbm in enumerate((dg_hbm, du_hbm, dd_hbm)):
        for h in range(2):
            own.append(
                pltpu.make_async_copy(
                    hbm.at[pl.ds(16 * h, 16)], dw.at[i, z, y, h], loc.at[2 * i + h]
                )
            )
    fetch = []
    for i, (hbm, ref) in enumerate(
        ((sg_hbm, sg), (su_hbm, su), (sd_hbm, sd), (eg_hbm.at[0], eg), (eu_hbm.at[0], eu), (ed_hbm.at[0], ed))
    ):
        fetch.append(pltpu.make_async_copy(hbm, ref, lw.at[i]))
    for c in own + fetch:
        c.start()

    scores = scores_ref[...]
    weight = scores / jnp.sum(scores, axis=-1, keepdims=True) * route_scale
    lanes = iota((16, 128), 1)
    spread = jnp.zeros((16, 128), F32)
    for k in range(6):
        spread = jnp.where(routes_ref[:, k : k + 1] == lanes, weight[:, k : k + 1], spread)
    wg[q] = spread
    xg[q] = x_ref[...]

    pl.semaphore_wait(barrier, 22)

    x_copies, w_copies = [], []
    for k in range(1, 8):
        w_copies.append(remote(wg.at[q], wg.at[q], w_s.at[k], w_r.at[k], base + mate(k)))
        x_copies.append(remote(x_ref, xg.at[q], x_s.at[k], x_r.at[k], base + mate(k)))
    for c in x_copies + w_copies:
        c.start()

    for c in own:
        c.wait()

    def ring(part, step):
        copies = []
        for half in range(2):
            for sign in range(2):
                away = 1 if sign == 0 else 3
                along_y = (half == 0) == (part == 0)
                dev = device(*(plane(0, away) if along_y else plane(away, 0)))
                back = 0 if step == 0 else (4 - away)
                zz, yy = plane(0, back) if along_y else plane(back, 0)
                cols = pl.ds(0, 1024) if step == 0 else pl.ds(512 * sign, 512)
                if part == 0:
                    block = dw.at[:, zz, yy, half, :, cols]
                elif along_y:
                    block = dw.at[:, :, yy, half, :, cols]
                else:
                    block = dw.at[:, zz, :, half, :, cols]
                i = part * 8 + step * 4 + half * 2 + sign
                copies.append(remote(block, block, d_s.at[i], d_r.at[i], dev))
        return copies

    rings = [ring(0, 0), ring(0, 1), ring(1, 0), ring(1, 1)]
    for c in rings[0]:
        c.start()

    for c in fetch[:3]:
        c.wait()
    xv = x_ref[...]
    hidden = (silu(dot(xv, sg[...])) * dot(xv, su[...])).astype(BF)
    shared = dot(hidden, sd[...])

    for c in rings[0]:
        c.wait_recv()
    for c in rings[1]:
        c.start()

    for c in w_copies:
        c.wait_recv()
    w_t = wg[...].reshape(128, 128).T
    before = (iota((128, 128), 0) < iota((128, 128), 1)) & (
        iota((128, 128), 0) // 16 == iota((128, 128), 1) // 16
    )
    rank = dot(jnp.where(w_t > 0, 1.0, 0.0).astype(BF), jnp.where(before, 1.0, 0.0).astype(BF))
    mine = iota((16, 8, 128), 1) == q
    w_p = jnp.sum(jnp.where(mine, w_t.reshape(16, 8, 128), 0.0), axis=1)
    r_p = jnp.sum(jnp.where(mine, rank.reshape(16, 8, 128), 0.0), axis=1)
    slot = iota((16, 16, 128), 1)
    tok = iota((16, 16, 128), 2)
    w_b = jnp.broadcast_to(w_p[:, None, :], (16, 16, 128))
    r_b = jnp.broadcast_to(r_p[:, None, :], (16, 16, 128))
    fits = (slot // 2 == tok // 16) & (r_b == (slot % 2).astype(F32))
    picked = jnp.where(fits, w_b, 0.0).reshape(256, 128)
    choose = jnp.where(picked > 0, 1.0, 0.0).astype(BF)
    combine = picked.T
    comb_hi = combine.astype(BF)
    comb_lo = (combine - comb_hi.astype(F32)).astype(BF)

    for c in x_copies:
        c.wait_recv()
    xall = xg[...].reshape(128, 1024)
    sbuf[...] = dot(choose, xall).astype(BF).reshape(4, 4, 16, 1024)
    out_copies = {}
    for dz, dy in offsets:
        zz, yy = plane(dz, dy)
        i = dz * 4 + dy
        out_copies[i] = remote(
            sbuf.at[zz, yy], rbuf.at[z, y], a_s.at[i], a_r.at[i], device(zz, yy)
        )
        out_copies[i].start()
    rbuf[z, y] = sbuf[z, y]

    for c in rings[1]:
        c.wait_recv()
    for c in rings[2]:
        c.start()

    for c in fetch[3:]:
        c.wait()
    back_copies = {}
    for dz in (0, 1, 3, 2):
        for dy in range(4):
            if (dz, dy) != (0, 0):
                out_copies[dz * 4 + dy].wait_recv()
        zz = lax.rem(z + 4 - dz, 4)
        rows = rbuf[zz].reshape(64, 1024)
        hid = (silu(dot(rows, eg[...])) * dot(rows, eu[...])).astype(BF)
        ybuf[zz] = dot(hid, ed[...]).astype(BF).reshape(4, 16, 1024)
        for dy in (0, 1, 3, 2):
            if (dz, dy) != (0, 0):
                yy = lax.rem(y + 4 - dy, 4)
                i = dz * 4 + dy
                back_copies[i] = remote(
                    ybuf.at[zz, yy], bbuf.at[z, y], b_s.at[i], b_r.at[i], device(zz, yy)
                )
                back_copies[i].start()
    bbuf[z, y] = ybuf[z, y]

    for c in rings[2]:
        c.wait_recv()
    for c in rings[3]:
        c.start()
    for c in rings[3]:
        c.wait_recv()

    gate = dot_t(xall, dw[0].reshape(512, 1024))
    up = dot_t(xall, dw[1].reshape(512, 1024))
    dense = dot((silu(gate) * up).astype(BF), dw[2].reshape(512, 1024))
    mix = mix_ref[...]
    partial = dense * (1.0 / (1.0 + jnp.exp(-mix)))

    for i in back_copies:
        back_copies[i].wait_recv()
    back = bbuf[...].reshape(256, 1024)
    partial = partial + dot(comb_hi, back) + dot(comb_lo, back)
    pbuf[...] = partial.astype(BF).reshape(8, 16, 1024)
    p_copies = []
    for k in range(1, 8):
        p_copies.append(
            remote(pbuf.at[mate(k)], qbuf.at[q], p_s.at[k], p_r.at[k], base + mate(k))
        )
    for c in p_copies:
        c.start()
    qbuf[q] = pbuf[q]
    for c in p_copies:
        c.wait_recv()
    total = shared + jnp.sum(qbuf[...].astype(F32), axis=0)
    out_ref[...] = (res_ref[...] + normed(total)).astype(BF)

    for c in w_copies + x_copies + p_copies:
        c.wait_send()
    for r in rings:
        for c in r:
            c.wait_send()
    for group in (out_copies, back_copies):
        for i in group:
            group[i].wait_send()


def exchange(x, residual, routes, scores, mix, eg, eu, ed, sg, su, sd, dg, du, dd):
    vm = pl.BlockSpec(memory_space=pltpu.VMEM)
    hbm = pl.BlockSpec(memory_space=pl.ANY)
    dma = pltpu.SemaphoreType.DMA
    return pl.pallas_call(
        ffn_kernel,
        out_shape=jax.ShapeDtypeStruct((16, 1024), BF),
        in_specs=[vm] * 5 + [hbm] * 9,
        out_specs=vm,
        scratch_shapes=[
            pltpu.VMEM((8, 16, 1024), BF),
            pltpu.VMEM((8, 16, 128), F32),
            pltpu.VMEM((3, 4, 4, 2, 16, 1024), BF),
            pltpu.VMEM((4, 4, 16, 1024), BF),
            pltpu.VMEM((4, 4, 16, 1024), BF),
            pltpu.VMEM((4, 4, 16, 1024), BF),
            pltpu.VMEM((4, 4, 16, 1024), BF),
            pltpu.VMEM((8, 16, 1024), BF),
            pltpu.VMEM((8, 16, 1024), BF),
            pltpu.VMEM((1024, 256), BF),
            pltpu.VMEM((1024, 256), BF),
            pltpu.VMEM((256, 1024), BF),
            pltpu.VMEM((1024, 256), BF),
            pltpu.VMEM((1024, 256), BF),
            pltpu.VMEM((256, 1024), BF),
            dma((6,)), dma((6,)), dma((8,)), dma((8,)), dma((16,)), dma((16,)),
            dma((8,)), dma((8,)), dma((16,)), dma((16,)), dma((16,)), dma((16,)),
            dma((8,)), dma((8,)),
        ],
        compiler_params=pltpu.CompilerParams(collective_id=0, has_side_effects=True),
    )(x, residual, routes, scores, mix, eg, eu, ed, sg, su, sd, dg, du, dd)


def per_device(
    tokens, lengths, cache_keys, cache_values, retention_state, mix_gain,
    query_weight, key_weight, value_weight, out_weight, ffn_gain, routes, route_scores,
    expert_gate, expert_up, expert_down, shared_gate, shared_up, shared_down,
    dense_gate, dense_up, dense_down, dense_mix,
):
    residual, new_keys, new_values = retain(
        tokens, lengths, mix_gain, query_weight, key_weight, value_weight, out_weight,
        cache_keys, cache_values, retention_state,
    )
    normal_ffn = (normed(residual) * ffn_gain).astype(BF)
    layer_out = exchange(
        normal_ffn, residual, routes, route_scores, dense_mix[None, :],
        expert_gate, expert_up, expert_down, shared_gate, shared_up, shared_down,
        dense_gate, dense_up, dense_down,
    )
    return (layer_out, new_keys, new_values)


def solution(mesh):
    row = P("ep", None)
    cube = P("ep", None, None)
    in_specs = (
        row, P("ep"), cube, cube, P("ep", None, None, None), P(), P(), P(), P(), P(), P(),
        row, row, cube, cube, cube, P(), P(), P(), row, row, row, P(),
    )
    return jax.shard_map(
        per_device, mesh=mesh, in_specs=in_specs, out_specs=(row, row, row), check_vma=False
    )
```

time: 144 us -> 76.7 us (0.53)
  Pallas kernels: 0 us -> 51 us
  waiting for transfers between devices: 40.4 us -> 0 us
  blocking collectives: 29.4 us -> 0 us
  matrix products: 37.7 us -> 13.3 us
  between operations: 14.3 us -> 0.84 us
  starting transfers between devices: 5.61 us -> 0 us
  other arithmetic: 8.52 us -> 3.73 us
    pallas_call x0 -> x1, Pallas kernels: none -> 51 us  [exchange(): pl.pallas_call(ffn_kernel, out_shape=jax.ShapeDtypeStruct((16, 1024), BF)...]
    all_to_all x1 -> x0, blocking collectives: 29.4 us -> none  [exchanged_experts(): lax.all_to_all(outgoing, 'ep', split_axis=0, concat_axis=0, tiled=True)]
    all_gather x1 -> x0, waiting for transfers between devices: 23.9 us -> none  [side_by_side(): lax.all_gather(both, axis, axis=dim, tiled=True)]
    dot_general x8 -> x0, matrix products: 22.8 us -> none  [the longest x1 9.86 us: dense_part(): return jnp.dot(hidden, down_rows, preferred_element_type=jnp.float32)]
    all_to_all x1 -> x0, waiting for transfers between devices: 16.5 us -> none  [exchanged_experts(): lax.all_to_all(outputs.reshape(arrived.shape), 'ep', split_axis=0, concat...]
    all_to_all x1 -> x0, starting transfers between devices: 5.58 us -> none  [exchanged_experts(): lax.all_to_all(outputs.reshape(arrived.shape), 'ep', split_axis=0, concat...]
    reshape x4 -> x0, local copies, waits for them, and re-layouts: 2.68 us -> none  [the longest x1 1.24 us: exchanged_experts(): arrived.reshape(-1, model_width)]
    unnamed x23 -> x25, local copies, waits for them, and re-layouts: 0.75 us -> 3.4 us
  transfers between devices with their start and end apart: 2 -> 0, of which waited for: 2 -> 0; matrix products, arithmetic and copies ran while one was open for 23% -> 0% of each run, Pallas kernels for 0% -> 0%
where the time goes in v1:
time: 76.7 us; the launch traced here: 76.3 us
  Pallas kernels  51 us (66%)
  matrix products  13.3 us (17%)
  local copies, waits for them, and re-layouts  7.38 us (10%)
  other arithmetic  3.73 us (5%)
  between operations  0.84 us (1%)
    pallas_call x1, Pallas kernels, exchange(): pl.pallas_call(ffn_kernel, out_shape=jax.ShapeDtypeStruct((16, 1024), BF)...  51 us
    dot_general x1, matrix products, retain(): jnp.einsum('shd,shde->she', queries.astype(jnp.float32), carry_state)  4.19 us
    reshape x1, local copies, waits for them, and re-layouts, retain(): cache_keys.reshape(seq_count, block_size, head_count, key_size)  3.91 us
    unnamed x25, local copies, waits for them, and re-layouts  3.4 us
    dot_general x1, matrix products, retain(): jnp.einsum('shj,sjhe->she', weighted, stored_values, preferred_element_ty...  2.84 us
    dot_general x1, matrix products, retain(): jnp.einsum('shd,sjhd->shj', queries, stored_keys, preferred_element_type=...  2.24 us
    dot_general x1, matrix products, retain(): jnp.dot(normal_in, w_query, preferred_element_type=jnp.float32)  1.55 us
    dot_general x1, matrix products, retain(): jnp.dot(normal_in, w_key, preferred_element_type=jnp.float32)  1.55 us

profile of v1, /device:TPU:1, one launch (start us, length us, event | category | flops | bytes accessed | tf_op | source)
XLA Modules:
  0.0 76.3 jit_solution(15391582348814288852)
XLA Ops:
  0.6 1.0 %fusion.3 = f32[16]{0:T(128)S(1)} fusion(bf16[16,1024]{1,0:T(8,128)(2,1)} %param.23), kind=kLoop, calls=%fused_computation.7 | loop fusion | flops 49136 | bytes 32832 | tf_op jit(solution)/shard_map/reduce_sum | solution.py:17
  1.7 1.6 %fusion.18 = f32[16,512]{1,0:T(8,128)S(1)} fusion(bf16[1024,512]{1,0:T(8,128)(2,1)} %param.29, bf16[16,1024]{1,0:T(8,128)(2,1)} %param.23, f32[1024]{0:T(1024)} %param.28, f32[16]{0:T(128)S(1)} %add_rsqrt_fusion.3), kind=kOutput, calls=%fused_computation.52 | convolution fusion | flops 16842752 | bytes 1118272 | tf_op jit(solution)/shard_map/dot_general | solution.py:45
  3.3 0.7 convert_element_type.73
  3.9 0.1 multiply_cosine_fusion
  4.1 0.1 multiply_subtract_fusion.1
  4.1 1.5 %fusion.16 = f32[16,512]{1,0:T(8,128)S(1)} fusion(bf16[1024,512]{1,0:T(8,128)(2,1)} %param.30, bf16[16,1024]{1,0:T(8,128)(2,1)} %param.23, f32[1024]{0:T(1024)} %param.28, f32[16]{0:T(128)S(1)} %add_rsqrt_fusion.3), kind=kOutput, calls=%fused_computation.51 | convolution fusion | flops 16842752 | bytes 1118272 | tf_op jit(solution)/shard_map/dot_general | solution.py:48
  5.7 0.1 multiply_subtract_fusion
  5.8 0.2 multiply_reduce_fusion.3
  6.0 3.9 %copy.35 = bf16[16,128,512]{1,2,0:T(8,128)(2,1)} copy(bf16[16,128,512]{2,1,0:T(8,128)(2,1)} %param.25) | data formatting | bytes 4194304 | tf_op jit(solution)/shard_map/reshape | solution.py:60
  9.9 2.2 %fusion.11 = f32[16,4,1,128]{3,2,1,0:T(1,128)S(1)} fusion(bf16[16,128,4,128]{1,3,2,0:T(8,128)(2,1)} %bitcast.34, bf16[16,4,128,1]{2,1,0,3:T(4,128)(2,1)S(1)} %bitcast.36), kind=kOutput, calls=%fused_computation.30 | convolution fusion | flops 2097152 | bytes 2146304 | tf_op jit(solution)/shard_map/shd,sjhd->shj/dot_general | solution.py:62
  12.4 0.1 fusion.13
  12.5 2.8 %fusion = f32[16,4,1,256]{3,2,1,0:T(1,128)S(1)} fusion(bf16[16,16,4,8,256]{4,3,2,1,0:T(8,128)(2,1)} %bitcast.35, bf16[16,4,128,1]{2,1,0,3:T(4,128)(2,1)S(1)} %fusion.13), kind=kOutput, calls=%fused_computation | convolution fusion | flops 4194304 | bytes 4276224 | tf_op jit(solution)/shard_map/shj,sjhe->she/dot_general | solution.py:73
  15.3 4.2 %fusion.9 = f32[16,4,1,256]{3,2,1,0:T(1,128)S(1)} fusion(f32[16,4,128,256]{3,2,1,0:T(8,128)} %param.27, bf16[16,4,128,1]{2,1,0,3:T(4,128)(2,1)S(1)} %bitcast.37), kind=kOutput, calls=%fused_computation.28 | convolution fusion | flops 4194304 | bytes 8470528 | tf_op jit(solution)/shard_map/shd,shde->she/dot_general | solution.py:77
  19.6 0.4 convolution_convert_fusion
  20.1 0.2 multiply_reduce_fusion.2
  20.3 0.1 multiply_convert_fusion.1
  20.4 0.5 multiply_reduce_fusion.1
  20.9 0.2 multiply_reduce_fusion
  21.2 0.7 multiply_convert_fusion.x_ref
  21.9 0.7 copy.26.routes_ref
  22.6 0.7 copy.27.scores_ref
  23.2 51.0 %shard_map.238 = bf16[16,1024]{1,0:T(8,128)(2,1)} custom-call(bf16[16,1024]{1,0:T(8,128)(2,1)} %multiply_convert_fusion.x_ref, f32[16,1024]{1,0:T(8,128)} %copy-done.3, s32[16,6]{1,0:T(8,128)} %copy.26.routes_ref, f32[16,6]{1,0:T(8,128)} %copy.27.scores_ref, f32[1,1024]{1,0:T(1,128)} %bitcast.43, bf16[1,1024,256]{2,1,0:T(8,128)(2,1)} %eg_hbm.1, ...), custom_call_target="tpu_custom_call" | custom-call | tf_op jit(solution)/shard_map/pallas_call | solution.py:324
  74.3 0.6 copy.54
  74.9 1.4 %copy.56 = bf16[16,1024]{1,0:T(8,128)(2,1)} copy(bf16[16,1024]{1,0:T(8,128)(2,1)} %shard_map.238) | data formatting | bytes 65536
  (35 shorter events, 0.4 us)
Async XLA Ops:
  0.6 19.8 %copy-start = (bf16[1024,1024]{1,0:T(8,128)(2,1)S(1)}, bf16[1024,1024]{1,0:T(8,128)(2,1)}, u32[]{:S(2)}) copy-start(bf16[1024,1024]{1,0:T(8,128)(2,1)} %param.32) | copy-start | bytes 6291460
  9.9 2.2 %copy-start.9 = (s32[16]{0:T(128)S(1)}, s32[16]{0:T(128)}, u32[]{:S(2)}) copy-start(s32[16]{0:T(128)} %param.24) | copy-start | bytes 196
  15.3 4.2 %copy-start.1 = (bf16[1024,1024]{1,0:T(8,128)(2,1)S(1)}, bf16[1024,1024]{1,0:T(8,128)(2,1)}, u32[]{:S(2)}) copy-start(bf16[1024,1024]{1,0:T(8,128)(2,1)} %param.31) | copy-start | bytes 6291460
  15.3 4.2 %copy-start.2 = (bf16[16,1024]{1,0:T(8,128)(2,1)S(1)}, bf16[16,1024]{1,0:T(8,128)(2,1)}, u32[]{:S(2)}) copy-start(bf16[16,1024]{1,0:T(8,128)(2,1)} %param.23) | copy-start | bytes 98308
  15.3 4.2 %copy-start.5 = (f32[1024]{0:T(1024)S(1)}, f32[1024]{0:T(1024)}, u32[]{:S(2)}) copy-start(f32[1024]{0:T(1024)} %param.28) | copy-start | bytes 12292
  19.5 1.6 %copy-start.6 = (f32[1024]{0:T(1024)S(1)}, f32[1024]{0:T(1024)}, u32[]{:S(2)}) copy-start(f32[1024]{0:T(1024)} %param.33) | copy-start | bytes 12292
  19.5 2.3 %copy-start.7 = (s32[16,6]{0,1:T(8,128)S(1)}, s32[16,6]{0,1:T(8,128)}, u32[]{:S(2)}) copy-start(s32[16,6]{0,1:T(8,128)} %param.34) | copy-start | bytes 1156
  19.6 3.0 %copy-start.8 = (f32[16,6]{0,1:T(8,128)S(1)}, f32[16,6]{0,1:T(8,128)}, u32[]{:S(2)}) copy-start(f32[16,6]{0,1:T(8,128)} %param.35) | copy-start | bytes 1156
  20.0 54.3 %copy-start.4 = (bf16[16,1024]{1,0:T(8,128)(2,1)}, bf16[16,1024]{1,0:T(8,128)(2,1)S(1)}, u32[]{:S(2)}) copy-start(bf16[16,1024]{1,0:T(8,128)(2,1)S(1)} %convolution_convert_fusion) | copy-start | bytes 98308
  21.1 2.1 %copy-start.3 = (f32[16,1024]{1,0:T(8,128)}, f32[16,1024]{1,0:T(8,128)S(1)}, u32[]{:S(2)}) copy-start(f32[16,1024]{1,0:T(8,128)S(1)} %get-tuple-element.4.res_ref) | copy-start | bytes 196612

commit v2 on v1

v2 whole, which is shorter than its diff:
```python
import math

import jax
import jax.numpy as jnp
from jax import lax
from jax.experimental import pallas as pl
from jax.experimental.pallas import tpu as pltpu
from jax.sharding import PartitionSpec as P

eps = 1e-06
route_scale = 2.5
rope_base = 10000.0
MESH = pl.DeviceIdType.MESH
BF = jnp.bfloat16
F32 = jnp.float32
scope = jax.named_scope


def normed(values):
    return values * lax.rsqrt(jnp.mean(values * values, axis=-1, keepdims=True) + eps)


def dot(a, b):
    return jnp.dot(a, b, preferred_element_type=F32)


def dot_t(a, b):
    return lax.dot_general(a, b, (((1,), (1,)), ((), ())), preferred_element_type=F32)


def silu(v):
    return v / (1.0 + jnp.exp(-v))


def iota(shape, dim):
    return lax.broadcasted_iota(jnp.int32, shape, dim)


def onehot(mask):
    return jnp.where(mask, 1.0, 0.0).astype(BF)


def sin_cos(angle):
    n = jnp.floor(angle * (2.0 / math.pi) + 0.5)
    r = ((angle - n * 1.5703125) - n * 4.837512969970703125e-4) - n * 7.54978995489188216e-8
    s2 = r * r
    sine = r + r * s2 * ((-1.9515295891e-4 * s2 + 8.3321608736e-3) * s2 - 1.6666654611e-1)
    cosine = 1.0 - 0.5 * s2 + s2 * s2 * (
        (2.443315711809948e-5 * s2 - 1.388731625493765e-3) * s2 + 4.166664568298827e-2
    )
    m = n - 4.0 * jnp.floor(n * 0.25)
    odd = (m == 1.0) | (m == 3.0)
    s_val = jnp.where(odd, cosine, sine)
    c_val = jnp.where(odd, sine, cosine)
    s_val = jnp.where(m >= 2.0, -s_val, s_val)
    c_val = jnp.where((m == 1.0) | (m == 2.0), -c_val, c_val)
    return s_val, c_val


def by_head(wide, rows):
    head = iota((rows, 256), 0) % 8
    total = jnp.zeros((rows, 256), F32)
    for h in range(4):
        total = jnp.where(head == h, wide[:, 256 * h : 256 * h + 256], total)
    return total


def layer_kernel(
    tok_hbm, len_hbm, gain_hbm, fgain_hbm, mix_hbm, routes_hbm, scores_hbm,
    wq_hbm, wk_hbm, wv_hbm, wo_hbm, ck_hbm, cv_hbm, st_hbm,
    eg_hbm, eu_hbm, ed_hbm, sg_hbm, su_hbm, sd_hbm, dg_hbm, du_hbm, dd_hbm,
    out_ref, keys_ref, vals_ref,
    tok_v, len_v, gain_v, fgain_v, mix_v, routes_v, scores_v,
    wq, wk, wv, wo, ck, cv, st,
    eg, eu, ed, sg, su, sd,
    xg, xown, wg, dw, sbuf, rbuf, ybuf, bbuf, pbuf, qbuf, qrows, decay_v, acc_v,
    loc, lw, w_s, w_r, d_s, d_r, x_s, x_r, a_s, a_r, b_s, b_r, p_s, p_r,
):
    me = lax.axis_index("ep")
    q = lax.rem(me, 8)
    p = lax.div(me, 8)
    z = lax.div(p, 4)
    y = lax.rem(p, 4)
    base = me - q

    def mate(k):
        return lax.rem(q + k, 8)

    def plane(dz, dy):
        return lax.rem(z + dz, 4), lax.rem(y + dy, 4)

    def device(zz, yy):
        return (zz * 4 + yy) * 8 + q

    def remote(src, dst, s, r, dev):
        return pltpu.make_async_remote_copy(
            src_ref=src, dst_ref=dst, send_sem=s, recv_sem=r, device_id=(dev,), device_id_type=MESH
        )

    barrier = pltpu.get_barrier_semaphore()
    for k in range(1, 8):
        pl.semaphore_signal(barrier, inc=1, device_id=(base + mate(k),), device_id_type=MESH)
    offsets = [(dz, dy) for dz in (0, 1, 3, 2) for dy in (0, 1, 3, 2) if (dz, dy) != (0, 0)]
    for dz, dy in offsets:
        pl.semaphore_signal(barrier, inc=1, device_id=(device(*plane(dz, dy)),), device_id_type=MESH)

    own = []
    for i, hbm in enumerate((dg_hbm, du_hbm, dd_hbm)):
        for h in range(2):
            own.append(
                pltpu.make_async_copy(
                    hbm.at[pl.ds(16 * h, 16)], dw.at[i, z, y, h], loc.at[2 * i + h]
                )
            )
    fetch = {}

    def want(name, hbm, ref):
        fetch[name] = pltpu.make_async_copy(hbm, ref, lw.at[len(fetch)])

    def ready(*names):
        for name in names:
            fetch[name].wait()

    want("tok", tok_hbm, tok_v)
    want("gain", gain_hbm, gain_v)
    want("len", len_hbm, len_v)
    want("routes", routes_hbm, routes_v)
    want("scores", scores_hbm, scores_v)
    want("wq", wq_hbm, wq)
    want("wk", wk_hbm, wk)
    want("wv", wv_hbm, wv)
    want("ck", ck_hbm, ck)
    for i in range(2):
        want(f"cv{i}", cv_hbm.at[pl.ds(8 * i, 8)], cv.at[pl.ds(8 * i, 8)])
    for i in range(4):
        want(f"st{i}", st_hbm.at[pl.ds(4 * i, 4)], st.at[pl.ds(4 * i, 4)])
    want("wo", wo_hbm, wo)
    want("fgain", fgain_hbm, fgain_v)
    want("sg", sg_hbm, sg)
    want("su", su_hbm, su)
    want("sd", sd_hbm, sd)
    want("eg", eg_hbm.at[0], eg)
    want("eu", eu_hbm.at[0], eu)
    want("ed", ed_hbm.at[0], ed)
    want("mix", mix_hbm, mix_v)
    for c in own:
        c.start()
    for name in fetch:
        fetch[name].start()

    def ring(part, step):
        copies = []
        for half in range(2):
            for sign in range(2):
                away = 1 if sign == 0 else 3
                along_y = (half == 0) == (part == 0)
                dev = device(*(plane(0, away) if along_y else plane(away, 0)))
                back = 0 if step == 0 else (4 - away)
                zz, yy = plane(0, back) if along_y else plane(back, 0)
                cols = pl.ds(0, 1024) if step == 0 else pl.ds(512 * sign, 512)
                if part == 0:
                    block = dw.at[:, zz, yy, half, :, cols]
                elif along_y:
                    block = dw.at[:, :, yy, half, :, cols]
                else:
                    block = dw.at[:, zz, :, half, :, cols]
                i = part * 8 + step * 4 + half * 2 + sign
                copies.append(remote(block, block, d_s.at[i], d_r.at[i], dev))
        return copies

    rings = [ring(0, 0), ring(0, 1), ring(1, 0), ring(1, 1)]

    with scope("route"):
        ready("routes", "scores")
        scores = scores_v[...]
        weight = scores / jnp.sum(scores, axis=0, keepdims=True) * route_scale
        chosen = routes_v[...]
        names = iota((128, 16), 0)
        spread = jnp.zeros((128, 16), F32)
        for k in range(6):
            spread = jnp.where(chosen[k : k + 1, :] == names, weight[k : k + 1, :], spread)
        spread = jnp.concatenate([spread, jnp.zeros((128, 112), F32)], axis=1).T
        wg[q] = spread[:16]

    with scope("qkv"):
        ready("tok", "gain", "len")
        tok = tok_v[...].astype(F32)
        xn = (normed(tok) * gain_v[...]).astype(BF)
        lens = jnp.broadcast_to(len_v[...].astype(F32), (16, 16))
        diag = iota((16, 16), 0) == iota((16, 16), 1)
        len_c = jnp.sum(jnp.where(diag, lens, 0.0), axis=1, keepdims=True)
        fill_c = len_c - 128.0 * jnp.floor(len_c * (1.0 / 128.0))
        lane = iota((16, 128), 1)
        inverse = jnp.exp((lane % 64).astype(F32) * (-math.log(rope_base) / 64.0))
        sine, cosine = sin_cos(len_c * inverse)
        sine = jnp.where(lane < 64, -sine, sine)
        ready("wq", "wk")
        raw_q = dot(xn, wq[...])
        raw_k = dot(xn, wk[...])

        def rotate(raw):
            parts = []
            for h in range(4):
                v = raw[:, 128 * h : 128 * h + 128]
                parts.append(v * cosine + pltpu.roll(v, 64, 1) * sine)
            return jnp.concatenate(parts, axis=1)

        queries = (rotate(raw_q) * 128.0 ** (-0.5)).astype(BF)
        new_keys = rotate(raw_k).astype(BF)
        keys_ref[...] = new_keys
        ready("wv")
        new_values = dot(xn, wv[...]).astype(BF)
        vals_ref[...] = new_values

    with scope("rows"):
        spread_rows = onehot(iota((128, 16), 0) // 8 == iota((128, 16), 1))
        head_512 = iota((128, 512), 0) % 8 == iota((128, 512), 1) // 128
        q_rows = jnp.where(head_512, dot(spread_rows, queries), 0.0)
        own_w = jnp.sum(q_rows * dot(spread_rows, new_keys), axis=-1, keepdims=True)
        own_w = own_w.astype(BF).astype(F32)
        qrows[...] = q_rows
        fill = dot(spread_rows, jnp.broadcast_to(fill_c, (16, 256)).astype(BF))
        row = iota((128, 256), 0)
        col = iota((128, 256), 1)
        head = row % 8
        rate = jnp.full((128, 256), math.log1p(-(2.0 ** -5)), F32)
        for h in range(1, 4):
            rate = jnp.where(head == h, math.log1p(-(2.0 ** (-5 - h))), rate)
        place = (col % 128).astype(F32)
        live = (place < fill) & (col // 128 == (row // 8) % 2)
        decay_v[...] = jnp.where(live, jnp.exp(jnp.maximum(fill - place, 0.0) * rate), 0.0)
        carry = jnp.exp((fill + 1.0) * rate)
        acc_v[...] = own_w * by_head(dot(spread_rows, new_values), 128)

    with scope("barrier"):
        pl.semaphore_wait(barrier, 22)
        w_copies = [
            remote(wg.at[q], wg.at[q], w_s.at[k], w_r.at[k], base + mate(k)) for k in range(1, 8)
        ]
        for c in own:
            c.wait()
        for c in rings[0]:
            c.start()
        for c in w_copies:
            c.start()

    with scope("scores"):
        ready("ck")
        weights = []
        for i in range(8):
            r = slice(16 * i, 16 * i + 16)
            got = dot_t(qrows[r].astype(BF), ck[2 * i : 2 * i + 2].reshape(256, 512))
            weights.append((got * decay_v[r]).astype(BF))

    with scope("ring1"):
        for c in rings[0]:
            c.wait_recv()
        for c in rings[1]:
            c.start()

    with scope("values"):
        for i in range(8):
            if i % 4 == 0:
                ready(f"cv{i // 4}")
            r = slice(16 * i, 16 * i + 16)
            got = dot(weights[i], cv[2 * i : 2 * i + 2].reshape(256, 1024))
            acc_v[r] = acc_v[r] + by_head(got, 16)

    with scope("state"):
        low = iota((16, 512), 0) < 8
        for i in range(8):
            if i % 2 == 0:
                ready(f"st{i // 2}")
            r = slice(16 * i, 16 * i + 16)
            rows = qrows[r]
            both = jnp.concatenate(
                [jnp.where(low, rows, 0.0), jnp.where(low, 0.0, rows)], axis=1
            ).astype(BF)
            got = dot(both, st[2 * i : 2 * i + 2].reshape(1024, 256).astype(BF))
            acc_v[r] = acc_v[r] + got * carry[r]

    with scope("ring2"):
        for c in rings[1]:
            c.wait_recv()
        for c in rings[2]:
            c.start()

    with scope("out"):
        headed = normed(acc_v[...]).astype(BF)
        ready("wo")
        mixed = jnp.zeros((16, 1024), F32)
        for h in range(4):
            pick = onehot(iota((16, 128), 1) == iota((16, 128), 0) * 8 + h)
            mixed = mixed + dot(dot(pick, headed).astype(BF), wo[256 * h : 256 * h + 256])
        residual = tok + normed(mixed)
        ready("fgain")
        xv = (normed(residual) * fgain_v[...]).astype(BF)
        xown[...] = xv
        xg[q] = xv
        x_copies = [
            remote(xown, xg.at[q], x_s.at[k], x_r.at[k], base + mate(k)) for k in range(1, 8)
        ]
        for c in x_copies:
            c.start()

    with scope("shared"):
        ready("sg", "su", "sd")
        hidden = (silu(dot(xv, sg[...])) * dot(xv, su[...])).astype(BF)
        shared = dot(hidden, sd[...])

    with scope("slots"):
        for c in w_copies:
            c.wait_recv()
        w_t = wg[...].reshape(128, 128).T
        before = (iota((128, 128), 0) < iota((128, 128), 1)) & (
            iota((128, 128), 0) // 16 == iota((128, 128), 1) // 16
        )
        rank = dot(onehot(w_t > 0), onehot(before))
        mine = iota((16, 8, 128), 1) == q
        w_p = jnp.sum(jnp.where(mine, w_t.reshape(16, 8, 128), 0.0), axis=1)
        r_p = jnp.sum(jnp.where(mine, rank.reshape(16, 8, 128), 0.0), axis=1)
        slot = iota((16, 16, 128), 1)
        mate_of = iota((16, 16, 128), 2) // 16
        w_b = jnp.broadcast_to(w_p[:, None, :], (16, 16, 128))
        r_b = jnp.broadcast_to(r_p[:, None, :], (16, 16, 128))
        fits = (slot // 2 == mate_of) & (r_b == (slot % 2).astype(F32))
        picked = jnp.where(fits, w_b, 0.0).reshape(256, 128)
        choose = onehot(picked > 0)
        combine = picked.T
        comb_hi = combine.astype(BF)
        comb_lo = (combine - comb_hi.astype(F32)).astype(BF)

    with scope("xwait"):
        for c in x_copies:
            c.wait_recv()
    with scope("send"):
        xall = xg[...].reshape(128, 1024)
        sbuf[...] = dot(choose, xall).astype(BF).reshape(4, 4, 16, 1024)
        out_copies = {}
        for dz, dy in offsets:
            zz, yy = plane(dz, dy)
            i = dz * 4 + dy
            out_copies[i] = remote(
                sbuf.at[zz, yy], rbuf.at[z, y], a_s.at[i], a_r.at[i], device(zz, yy)
            )
            out_copies[i].start()
        rbuf[z, y] = sbuf[z, y]

    with scope("ring3"):
        for c in rings[2]:
            c.wait_recv()
        for c in rings[3]:
            c.start()

    ready("eg", "eu", "ed")
    back_copies = {}
    for dz in (0, 1, 3, 2):
        with scope(f"ewait{dz}"):
            for dy in range(4):
                if (dz, dy) != (0, 0):
                    out_copies[dz * 4 + dy].wait_recv()
        with scope(f"expert{dz}"):
            zz = lax.rem(z + 4 - dz, 4)
            rows = rbuf[zz].reshape(64, 1024)
            hid = (silu(dot(rows, eg[...])) * dot(rows, eu[...])).astype(BF)
            ybuf[zz] = dot(hid, ed[...]).astype(BF).reshape(4, 16, 1024)
            for dy in (0, 1, 3, 2):
                if (dz, dy) != (0, 0):
                    yy = lax.rem(y + 4 - dy, 4)
                    i = dz * 4 + dy
                    back_copies[i] = remote(
                        ybuf.at[zz, yy], bbuf.at[z, y], b_s.at[i], b_r.at[i], device(zz, yy)
                    )
                    back_copies[i].start()
    bbuf[z, y] = ybuf[z, y]

    with scope("dwait"):
        for c in rings[3]:
            c.wait_recv()

    with scope("dense"):
        gate = dot_t(xall, dw[0].reshape(512, 1024))
        up = dot_t(xall, dw[1].reshape(512, 1024))
        dense = dot((silu(gate) * up).astype(BF), dw[2].reshape(512, 1024))
        ready("mix")
        partial = dense * (1.0 / (1.0 + jnp.exp(-mix_v[...])))

    with scope("bwait"):
        for i in back_copies:
            back_copies[i].wait_recv()
    with scope("combine"):
        back = bbuf[...].reshape(256, 1024)
        partial = partial + dot(comb_hi, back) + dot(comb_lo, back)
        pbuf[...] = partial.astype(BF).reshape(8, 16, 1024)
        p_copies = []
        for k in range(1, 8):
            p_copies.append(
                remote(pbuf.at[mate(k)], qbuf.at[q], p_s.at[k], p_r.at[k], base + mate(k))
            )
        for c in p_copies:
            c.start()
        qbuf[q] = pbuf[q]
    with scope("pwait"):
        for c in p_copies:
            c.wait_recv()
    with scope("final"):
        total = shared + jnp.sum(qbuf[...].astype(F32), axis=0)
        out_ref[...] = (residual + normed(total)).astype(BF)

    with scope("drain"):
        for c in w_copies + x_copies + p_copies:
            c.wait_send()
        for r in rings:
            for c in r:
                c.wait_send()
        for group in (out_copies, back_copies):
            for i in group:
                group[i].wait_send()


def per_device(
    tokens, lengths, cache_keys, cache_values, retention_state, mix_gain,
    query_weight, key_weight, value_weight, out_weight, ffn_gain, routes, route_scores,
    expert_gate, expert_up, expert_down, shared_gate, shared_up, shared_down,
    dense_gate, dense_up, dense_down, dense_mix,
):
    vm = pl.BlockSpec(memory_space=pltpu.VMEM)
    hbm = pl.BlockSpec(memory_space=pl.ANY)
    dma = pltpu.SemaphoreType.DMA
    args = (
        tokens, lengths[None, :], mix_gain[None, :], ffn_gain[None, :], dense_mix[None, :],
        routes.T, route_scores.T,
        query_weight, key_weight, value_weight, out_weight,
        cache_keys, cache_values, retention_state.reshape(16, 512, 256),
        expert_gate, expert_up, expert_down, shared_gate, shared_up, shared_down,
        dense_gate, dense_up, dense_down,
    )
    local = [a.shape for a in args[:14]] + [a.shape[-2:] for a in args[14:20]]
    return pl.pallas_call(
        layer_kernel,
        out_shape=(
            jax.ShapeDtypeStruct((16, 1024), BF),
            jax.ShapeDtypeStruct((16, 512), BF),
            jax.ShapeDtypeStruct((16, 1024), BF),
        ),
        in_specs=[hbm] * len(args),
        out_specs=(vm, vm, vm),
        scratch_shapes=[pltpu.VMEM(s, a.dtype) for s, a in zip(local, args)]
        + [
            pltpu.VMEM((8, 16, 1024), BF),
            pltpu.VMEM((16, 1024), BF),
            pltpu.VMEM((8, 16, 128), F32),
            pltpu.VMEM((3, 4, 4, 2, 16, 1024), BF),
            pltpu.VMEM((4, 4, 16, 1024), BF),
            pltpu.VMEM((4, 4, 16, 1024), BF),
            pltpu.VMEM((4, 4, 16, 1024), BF),
            pltpu.VMEM((4, 4, 16, 1024), BF),
            pltpu.VMEM((8, 16, 1024), BF),
            pltpu.VMEM((8, 16, 1024), BF),
            pltpu.VMEM((128, 512), F32),
            pltpu.VMEM((128, 256), F32),
            pltpu.VMEM((128, 256), F32),
            dma((6,)), dma((24,)), dma((8,)), dma((8,)), dma((16,)), dma((16,)),
            dma((8,)), dma((8,)), dma((16,)), dma((16,)), dma((16,)), dma((16,)),
            dma((8,)), dma((8,)),
        ],
        compiler_params=pltpu.CompilerParams(collective_id=0, has_side_effects=True),
    )(*args)


def solution(mesh):
    row = P("ep", None)
    cube = P("ep", None, None)
    in_specs = (
        row, P("ep"), cube, cube, P("ep", None, None, None), P(), P(), P(), P(), P(), P(),
        row, row, cube, cube, cube, P(), P(), P(), row, row, row, P(),
    )
    return jax.shard_map(
        per_device, mesh=mesh, in_specs=in_specs, out_specs=(row, row, row), check_vma=False
    )
```

time: 76.7 us -> 60.6 us (0.79)
  matrix products: 13.3 us -> 0 us
  Pallas kernels: 51 us -> 55.5 us
  other arithmetic: 3.73 us -> 0 us
  local copies, waits for them, and re-layouts: 7.38 us -> 4.07 us
    dot_general x7 -> x0, matrix products: 13.3 us -> none  [the longest x1 4.19 us: retain(): jnp.einsum('shd,shde->she', queries.astype(jnp.float32), carry_state)]
    pallas_call x1, Pallas kernels: 51 us -> 55.5 us  [per_device(): pl.pallas_call(layer_kernel, out_shape=(jax.ShapeDtypeStruct((16, 1024),...]
    reshape x3 -> x0, local copies, waits for them, and re-layouts: 3.94 us -> none  [the longest x1 3.91 us: retain(): cache_keys.reshape(seq_count, block_size, head_count, key_size)]
    convert_element_type x6 -> x0, other arithmetic: 1.61 us -> none  [the longest x1 0.69 us: per_device(): normal_ffn = (normed(residual) * ffn_gain).astype(BF)]
    reduce_sum x4 -> x0, other arithmetic: 1.6 us -> none  [the longest x3 1.41 us: normed(): jnp.mean(values * values, axis=-1, keepdims=True) + eps]
    unnamed x25 -> x3, local copies, waits for them, and re-layouts: 3.4 us -> 4.07 us
where the time goes in v2:
time: 60.6 us; the launch traced here: 60.3 us
  Pallas kernels  55.5 us (92%)
  local copies, waits for them, and re-layouts  4.07 us (7%)
  between operations  0.65 us (1%)
    pallas_call x1, Pallas kernels, per_device(): pl.pallas_call(layer_kernel, out_shape=(jax.ShapeDtypeStruct((16, 1024),...  55.5 us
    unnamed x3, local copies, waits for them, and re-layouts  4.07 us

profile of v2, /device:TPU:1, one launch (start us, length us, event | category | flops | bytes accessed | tf_op | source)
XLA Modules:
  0.0 60.3 jit_solution(3308557091740469371)
XLA Ops:
  0.6 55.5 %shard_map.238 = (bf16[16,1024]{1,0:T(8,128)(2,1)}, bf16[16,512]{1,0:T(8,128)(2,1)}, bf16[16,1024]{1,0:T(8,128)(2,1)}) custom-call(bf16[16,1024]{1,0:T(8,128)(2,1)} %tok_hbm.1, s32[1,16]{1,0:T(1,128)} %bitcast.13, f32[1,1024]{1,0:T(1,128)} %bitcast.8, f32[1,1024]{1,0:T(1,128)} %bitcast.9, f32[1,1024]{1,0:T(1,128)} %bitcast.10, s32[6,16]{1,0:T(8,128)} %bitcast.11, ...), custom_call_target="tpu_custom_call" | custom-call | tf_op jit(solution)/shard_map/pallas_call | solution.py:439
  56.2 1.4 %copy.29 = bf16[16,1024]{1,0:T(8,128)(2,1)} copy(bf16[16,1024]{1,0:T(8,128)(2,1)} %get-tuple-element.6) | data formatting | bytes 65536
  57.6 1.3 %copy.30 = bf16[16,512]{1,0:T(8,128)(2,1)} copy(bf16[16,512]{1,0:T(8,128)(2,1)} %get-tuple-element.7) | data formatting | bytes 32768
  58.9 1.4 %copy.31 = bf16[16,1024]{1,0:T(8,128)(2,1)} copy(bf16[16,1024]{1,0:T(8,128)(2,1)} %get-tuple-element.8) | data formatting | bytes 65536

commit v3 on v2

--- a/solution.py
+++ b/solution.py
@@ -73,7 +73,7 @@
     tok_v, len_v, gain_v, fgain_v, mix_v, routes_v, scores_v,
     wq, wk, wv, wo, ck, cv, st,
     eg, eu, ed, sg, su, sd,
-    xg, xown, wg, dw, sbuf, rbuf, ybuf, bbuf, pbuf, qbuf, qrows, decay_v, acc_v,
+    xg, xown, wg, wt, dw, dense_v, sbuf, rbuf, ybuf, bbuf, pbuf, qbuf, qrows, decay_v, acc_v,
     loc, lw, w_s, w_r, d_s, d_r, x_s, x_r, a_s, a_r, b_s, b_r, p_s, p_r,
 ):
     me = lax.axis_index("ep")
@@ -82,6 +82,7 @@
     z = lax.div(p, 4)
     y = lax.rem(p, 4)
     base = me - q
+    other = q + 1 - 2 * lax.rem(q, 2)
 
     def mate(k):
         return lax.rem(q + k, 8)
@@ -106,12 +107,7 @@
 
     own = []
     for i, hbm in enumerate((dg_hbm, du_hbm, dd_hbm)):
-        for h in range(2):
-            own.append(
-                pltpu.make_async_copy(
-                    hbm.at[pl.ds(16 * h, 16)], dw.at[i, z, y, h], loc.at[2 * i + h]
-                )
-            )
+        own.append(pltpu.make_async_copy(hbm, dw.at[i, q], loc.at[i]))
     fetch = {}
 
     def want(name, hbm, ref):
@@ -148,27 +144,14 @@
     for name in fetch:
         fetch[name].start()
 
-    def ring(part, step):
-        copies = []
-        for half in range(2):
-            for sign in range(2):
-                away = 1 if sign == 0 else 3
-                along_y = (half == 0) == (part == 0)
-                dev = device(*(plane(0, away) if along_y else plane(away, 0)))
-                back = 0 if step == 0 else (4 - away)
-                zz, yy = plane(0, back) if along_y else plane(back, 0)
-                cols = pl.ds(0, 1024) if step == 0 else pl.ds(512 * sign, 512)
-                if part == 0:
-                    block = dw.at[:, zz, yy, half, :, cols]
-                elif along_y:
-                    block = dw.at[:, :, yy, half, :, cols]
-                else:
-                    block = dw.at[:, zz, :, half, :, cols]
-                i = part * 8 + step * 4 + half * 2 + sign
-                copies.append(remote(block, block, d_s.at[i], d_r.at[i], dev))
-        return copies
-
-    rings = [ring(0, 0), ring(0, 1), ring(1, 0), ring(1, 1)]
+    def shard(i, which, to):
+        block = dw.at[:, which]
+        return remote(block, block, d_s.at[i], d_r.at[i], base + to)
+
+    along = [mate(2 * k) for k in range(1, 4)]
+    first = [shard(k, q, along[k]) for k in range(3)]
+    across = [shard(3, q, other)]
+    second = [shard(4 + k, along[k], other) for k in range(3)]
 
     with scope("route"):
         ready("routes", "scores")
@@ -180,7 +163,7 @@
         for k in range(6):
             spread = jnp.where(chosen[k : k + 1, :] == names, weight[k : k + 1, :], spread)
         spread = jnp.concatenate([spread, jnp.zeros((128, 112), F32)], axis=1).T
-        wg[q] = spread[:16]
+        wg[z, y] = spread[:16]
 
     with scope("qkv"):
         ready("tok", "gain", "len")
@@ -232,18 +215,6 @@
         carry = jnp.exp((fill + 1.0) * rate)
         acc_v[...] = own_w * by_head(dot(spread_rows, new_values), 128)
 
-    with scope("barrier"):
-        pl.semaphore_wait(barrier, 22)
-        w_copies = [
-            remote(wg.at[q], wg.at[q], w_s.at[k], w_r.at[k], base + mate(k)) for k in range(1, 8)
-        ]
-        for c in own:
-            c.wait()
-        for c in rings[0]:
-            c.start()
-        for c in w_copies:
-            c.start()
-
     with scope("scores"):
         ready("ck")
         weights = []
@@ -251,12 +222,6 @@
             r = slice(16 * i, 16 * i + 16)
             got = dot_t(qrows[r].astype(BF), ck[2 * i : 2 * i + 2].reshape(256, 512))
             weights.append((got * decay_v[r]).astype(BF))
-
-    with scope("ring1"):
-        for c in rings[0]:
-            c.wait_recv()
-        for c in rings[1]:
-            c.start()
 
     with scope("values"):
         for i in range(8):
@@ -279,10 +244,18 @@
             got = dot(both, st[2 * i : 2 * i + 2].reshape(1024, 256).astype(BF))
             acc_v[r] = acc_v[r] + got * carry[r]
 
-    with scope("ring2"):
-        for c in rings[1]:
-            c.wait_recv()
-        for c in rings[2]:
+    with scope("barrier"):
+        pl.semaphore_wait(barrier, 22)
+        w_copies = {}
+        for dz, dy in offsets:
+            i = dz * 4 + dy
+            w_copies[i] = remote(
+                wg.at[z, y], wg.at[z, y], w_s.at[i], w_r.at[i], device(*plane(dz, dy))
+            )
+            w_copies[i].start()
+        for c in own:
+            c.wait()
+        for c in first + across:
             c.start()
 
     with scope("out"):
@@ -296,126 +269,139 @@
         ready("fgain")
         xv = (normed(residual) * fgain_v[...]).astype(BF)
         xown[...] = xv
-        xg[q] = xv
-        x_copies = [
-            remote(xown, xg.at[q], x_s.at[k], x_r.at[k], base + mate(k)) for k in range(1, 8)
-        ]
-        for c in x_copies:
-            c.start()
+        xg[z, y] = xv
+        x_copies = {}
+        for dz, dy in offsets:
+            i = dz * 4 + dy
+            x_copies[i] = remote(xown, xg.at[z, y], x_s.at[i], x_r.at[i], device(*plane(dz, dy)))
+            x_copies[i].start()
 
     with scope("shared"):
         ready("sg", "su", "sd")
         hidden = (silu(dot(xv, sg[...])) * dot(xv, su[...])).astype(BF)
         shared = dot(hidden, sd[...])
 
-    with scope("slots"):
-        for c in w_copies:
-            c.wait_recv()
-        w_t = wg[...].reshape(128, 128).T
-        before = (iota((128, 128), 0) < iota((128, 128), 1)) & (
-            iota((128, 128), 0) // 16 == iota((128, 128), 1) // 16
-        )
-        rank = dot(onehot(w_t > 0), onehot(before))
-        mine = iota((16, 8, 128), 1) == q
-        w_p = jnp.sum(jnp.where(mine, w_t.reshape(16, 8, 128), 0.0), axis=1)
-        r_p = jnp.sum(jnp.where(mine, rank.reshape(16, 8, 128), 0.0), axis=1)
-        slot = iota((16, 16, 128), 1)
-        mate_of = iota((16, 16, 128), 2) // 16
-        w_b = jnp.broadcast_to(w_p[:, None, :], (16, 16, 128))
-        r_b = jnp.broadcast_to(r_p[:, None, :], (16, 16, 128))
-        fits = (slot // 2 == mate_of) & (r_b == (slot % 2).astype(F32))
-        picked = jnp.where(fits, w_b, 0.0).reshape(256, 128)
-        choose = onehot(picked > 0)
-        combine = picked.T
-        comb_hi = combine.astype(BF)
-        comb_lo = (combine - comb_hi.astype(F32)).astype(BF)
-
-    with scope("xwait"):
-        for c in x_copies:
-            c.wait_recv()
-    with scope("send"):
-        xall = xg[...].reshape(128, 1024)
-        sbuf[...] = dot(choose, xall).astype(BF).reshape(4, 4, 16, 1024)
-        out_copies = {}
-        for dz, dy in offsets:
-            zz, yy = plane(dz, dy)
-            i = dz * 4 + dy
-            out_copies[i] = remote(
-                sbuf.at[zz, yy], rbuf.at[z, y], a_s.at[i], a_r.at[i], device(zz, yy)
-            )
-            out_copies[i].start()
-        rbuf[z, y] = sbuf[z, y]
-
-    with scope("ring3"):
-        for c in rings[2]:
-            c.wait_recv()
-        for c in rings[3]:
-            c.start()
+    order = (0, 1, 3, 2)
+    before = onehot(
+        (iota((128, 128), 0) < iota((128, 128), 1))
+        & (iota((128, 128), 0) // 16 == iota((128, 128), 1) // 16)
+    )
+    slot = iota((8, 8, 128), 1)
+    sender = iota((8, 8, 128), 2) // 16
+    out_copies, picks, rows_of = {}, {}, {}
+    for dz in order:
+        zz = lax.rem(z + 4 - dz, 4)
+        rows_of[dz] = zz
+        with scope(f"xwait{dz}"):
+            for dy in range(4):
+                if (dz, dy) != (0, 0):
+                    w_copies[dz * 4 + dy].wait_recv()
+                    x_copies[dz * 4 + dy].wait_recv()
+        with scope(f"send{dz}"):
+            w_all = jnp.concatenate([wg[zz].reshape(64, 128), jnp.zeros((64, 128), F32)], axis=0)
+            wt[dz] = w_all.T
+            w_p = wt[dz, pl.ds(pl.multiple_of(p * 8, 8), 8), :]
+            r_p = dot(onehot(w_p > 0), before)
+            w_b = jnp.broadcast_to(w_p[:, None, :], (8, 8, 128))
+            r_b = jnp.broadcast_to(r_p[:, None, :], (8, 8, 128))
+            fits = (slot // 2 == sender) & (r_b == (slot % 2).astype(F32))
+            picked = jnp.where(fits, w_b, 0.0).reshape(64, 128)
+            picks[dz] = picked
+            choose = onehot(picked > 0)[:, :64]
+            sbuf[zz] = dot(choose, xg[zz].reshape(64, 1024)).astype(BF).reshape(8, 8, 1024)
+            for k in range(1, 8):
+                i = dz * 8 + k
+                out_copies[i] = remote(
+                    sbuf.at[zz, mate(k)], rbuf.at[zz, q], a_s.at[i], a_r.at[i], base + mate(k)
+                )
+                out_copies[i].start()
+            rbuf[zz, q] = sbuf[zz, q]
+
+    with scope("dfwd"):
+        for k in range(3):
+            first[k].wait_recv()
+            second[2 - k].start()
 
     ready("eg", "eu", "ed")
     back_copies = {}
-    for dz in (0, 1, 3, 2):
+    for dz in order:
+        zz = rows_of[dz]
         with scope(f"ewait{dz}"):
-            for dy in range(4):
-                if (dz, dy) != (0, 0):
-                    out_copies[dz * 4 + dy].wait_recv()
+            for k in range(1, 8):
+                out_copies[dz * 8 + k].wait_recv()
         with scope(f"expert{dz}"):
-            zz = lax.rem(z + 4 - dz, 4)
             rows = rbuf[zz].reshape(64, 1024)
             hid = (silu(dot(rows, eg[...])) * dot(rows, eu[...])).astype(BF)
-            ybuf[zz] = dot(hid, ed[...]).astype(BF).reshape(4, 16, 1024)
+            ybuf[zz] = dot(hid, ed[...]).astype(BF).reshape(8, 8, 1024)
+            for k in range(1, 8):
+                i = dz * 8 + k
+                back_copies[i] = remote(
+                    ybuf.at[zz, mate(k)], bbuf.at[zz, q], b_s.at[i], b_r.at[i], base + mate(k)
+                )
+                back_copies[i].start()
+            bbuf[zz, q] = ybuf[zz, q]
+
+    with scope("dwait"):
+        for c in across + second:
+            c.wait_recv()
+
+    with scope("dense"):
+        tokens = xg[...].reshape(256, 1024)
+        gate = dot_t(tokens, dw[0].reshape(256, 1024))
+        up = dot_t(tokens, dw[1].reshape(256, 1024))
+        ready("mix")
+        mix = 1.0 / (1.0 + jnp.exp(-mix_v[...]))
+        down = dw[2].reshape(256, 1024)
+        dense_v[...] = (dot((silu(gate) * up).astype(BF), down) * mix).reshape(4, 64, 1024)
+
+    p_copies = {}
+    for dz in order:
+        zz = rows_of[dz]
+        with scope(f"bwait{dz}"):
+            for k in range(1, 8):
+                back_copies[dz * 8 + k].wait_recv()
+        with scope(f"combine{dz}"):
+            combine = picks[dz].T[:64]
+            comb_hi = combine.astype(BF)
+            comb_lo = (combine - comb_hi.astype(F32)).astype(BF)
+            back = bbuf[zz].reshape(64, 1024)
+            partial = dense_v[zz] + dot(comb_hi, back) + dot(comb_lo, back)
+            pbuf[zz] = partial.astype(BF).reshape(4, 16, 1024)
             for dy in (0, 1, 3, 2):
                 if (dz, dy) != (0, 0):
                     yy = lax.rem(y + 4 - dy, 4)
                     i = dz * 4 + dy
-                    back_copies[i] = remote(
-                        ybuf.at[zz, yy], bbuf.at[z, y], b_s.at[i], b_r.at[i], device(zz, yy)
+                    p_copies[i] = remote(
+                        pbuf.at[zz, yy], qbuf.at[z, y], p_s.at[i], p_r.at[i], device(zz, yy)
                     )
-                    back_copies[i].start()
-    bbuf[z, y] = ybuf[z, y]
-
-    with scope("dwait"):
-        for c in rings[3]:
-            c.wait_recv()
-
-    with scope("dense"):
-        gate = dot_t(xall, dw[0].reshape(512, 1024))
-        up = dot_t(xall, dw[1].reshape(512, 1024))
-        dense = dot((silu(gate) * up).astype(BF), dw[2].reshape(512, 1024))
-        ready("mix")
-        partial = dense * (1.0 / (1.0 + jnp.exp(-mix_v[...])))
-
-    with scope("bwait"):
-        for i in back_copies:
-            back_copies[i].wait_recv()
-    with scope("combine"):
-        back = bbuf[...].reshape(256, 1024)
-        partial = partial + dot(comb_hi, back) + dot(comb_lo, back)
-        pbuf[...] = partial.astype(BF).reshape(8, 16, 1024)
-        p_copies = []
-        for k in range(1, 8):
-            p_copies.append(
-                remote(pbuf.at[mate(k)], qbuf.at[q], p_s.at[k], p_r.at[k], base + mate(k))
-            )
-        for c in p_copies:
-            c.start()
-        qbuf[q] = pbuf[q]
+                    p_copies[i].start()
+    qbuf[z, y] = pbuf[z, y]
     with scope("pwait"):
-        for c in p_copies:
-            c.wait_recv()
+        for i in p_copies:
+            p_copies[i].wait_recv()
     with scope("final"):
-        total = shared + jnp.sum(qbuf[...].astype(F32), axis=0)
+        total = shared + jnp.sum(qbuf[...].reshape(16, 16, 1024).astype(F32), axis=0)
         out_ref[...] = (residual + normed(total)).astype(BF)
 
     with scope("drain"):
-        for c in w_copies + x_copies + p_copies:
+        for c in first + across + second:
             c.wait_send()
-        for r in rings:
-            for c in r:
-                c.wait_send()
-        for group in (out_copies, back_copies):
+        for group in (w_copies, x_copies, out_copies, back_copies, p_copies):
             for i in group:
                 group[i].wait_send()
+
+
+def results_kernel(a_in, b_in, c_in, a_out, b_out, c_out, a_v, b_v, c_v, in_s, out_s):
+    trio = ((a_in, a_v, a_out), (b_in, b_v, b_out), (c_in, c_v, c_out))
+    loads = [pltpu.make_async_copy(i, v, in_s.at[n]) for n, (i, v, _) in enumerate(trio)]
+    stores = [pltpu.make_async_copy(v, o, out_s.at[n]) for n, (_, v, o) in enumerate(trio)]
+    for c in loads:
+        c.start()
+    for load, store in zip(loads, stores):
+        load.wait()
+        store.start()
+    for c in stores:
+        c.wait()
 
 
 def per_device(
@@ -436,36 +422,42 @@
         dense_gate, dense_up, dense_down,
     )
     local = [a.shape for a in args[:14]] + [a.shape[-2:] for a in args[14:20]]
-    return pl.pallas_call(
+    shapes = tuple(jax.ShapeDtypeStruct((16, n), BF) for n in (1024, 512, 1024))
+    held = pl.pallas_call(
         layer_kernel,
-        out_shape=(
-            jax.ShapeDtypeStruct((16, 1024), BF),
-            jax.ShapeDtypeStruct((16, 512), BF),
-            jax.ShapeDtypeStruct((16, 1024), BF),
-        ),
+        out_shape=shapes,
         in_specs=[hbm] * len(args),
         out_specs=(vm, vm, vm),
         scratch_shapes=[pltpu.VMEM(s, a.dtype) for s, a in zip(local, args)]
         + [
-            pltpu.VMEM((8, 16, 1024), BF),
+            pltpu.VMEM((4, 4, 16, 1024), BF),
             pltpu.VMEM((16, 1024), BF),
-            pltpu.VMEM((8, 16, 128), F32),
-            pltpu.VMEM((3, 4, 4, 2, 16, 1024), BF),
+            pltpu.VMEM((4, 4, 16, 128), F32),
+            pltpu.VMEM((4, 128, 128), F32),
+            pltpu.VMEM((3, 8, 32, 1024), BF),
+            pltpu.VMEM((4, 64, 1024), F32),
+            pltpu.VMEM((4, 8, 8, 1024), BF),
+            pltpu.VMEM((4, 8, 8, 1024), BF),
+            pltpu.VMEM((4, 8, 8, 1024), BF),
+            pltpu.VMEM((4, 8, 8, 1024), BF),
             pltpu.VMEM((4, 4, 16, 1024), BF),
             pltpu.VMEM((4, 4, 16, 1024), BF),
-            pltpu.VMEM((4, 4, 16, 1024), BF),
-            pltpu.VMEM((4, 4, 16, 1024), BF),
-            pltpu.VMEM((8, 16, 1024), BF),
-            pltpu.VMEM((8, 16, 1024), BF),
             pltpu.VMEM((128, 512), F32),
             pltpu.VMEM((128, 256), F32),
             pltpu.VMEM((128, 256), F32),
-            dma((6,)), dma((24,)), dma((8,)), dma((8,)), dma((16,)), dma((16,)),
-            dma((8,)), dma((8,)), dma((16,)), dma((16,)), dma((16,)), dma((16,)),
-            dma((8,)), dma((8,)),
+            dma((3,)), dma((24,)), dma((16,)), dma((16,)), dma((8,)), dma((8,)),
+            dma((16,)), dma((16,)), dma((32,)), dma((32,)), dma((32,)), dma((32,)),
+            dma((16,)), dma((16,)),
         ],
         compiler_params=pltpu.CompilerParams(collective_id=0, has_side_effects=True),
     )(*args)
+    return pl.pallas_call(
+        results_kernel,
+        out_shape=shapes,
+        in_specs=[hbm] * 3,
+        out_specs=(hbm,) * 3,
+        scratch_shapes=[pltpu.VMEM(a.shape, BF) for a in shapes] + [dma((3,)), dma((3,))],
+    )(*held)
 
 
 def solution(mesh):

time: 60.6 us -> 47.7 us (0.79)
  Pallas kernels: 55.5 us -> 46.9 us
  local copies, waits for them, and re-layouts: 4.07 us -> 0 us
    pallas_call x1 -> x2, Pallas kernels: 55.5 us -> 46.9 us  [the longest x1 45.4 us: per_device(): pl.pallas_call(layer_kernel, out_shape=shapes, in_specs=[hbm] * len(args)...]
    unnamed x3 -> x0, local copies, waits for them, and re-layouts: 4.07 us -> none
where the time goes in v3:
time: 47.7 us; the launch traced here: 47.5 us
  Pallas kernels  46.9 us (98%)
  between operations  0.65 us (1%)
    pallas_call x1, Pallas kernels, per_device(): pl.pallas_call(layer_kernel, out_shape=shapes, in_specs=[hbm] * len(args)...  45.4 us
    pallas_call x1, Pallas kernels, per_device(): pl.pallas_call(results_kernel, out_shape=shapes, in_specs=[hbm] * 3, out_...  1.46 us

profile of v3, /device:TPU:1, one launch (start us, length us, event | category | flops | bytes accessed | tf_op | source)
XLA Modules:
  0.0 47.5 jit_solution(7157653400095503838)
XLA Ops:
  0.6 45.4 %shard_map.238 = (bf16[16,1024]{1,0:T(8,128)(2,1)}, bf16[16,512]{1,0:T(8,128)(2,1)}, bf16[16,1024]{1,0:T(8,128)(2,1)}) custom-call(bf16[16,1024]{1,0:T(8,128)(2,1)} %tok_hbm.1, s32[1,16]{1,0:T(1,128)} %bitcast.13, f32[1,1024]{1,0:T(1,128)} %bitcast.8, f32[1,1024]{1,0:T(1,128)} %bitcast.9, f32[1,1024]{1,0:T(1,128)} %bitcast.10, s32[6,16]{1,0:T(8,128)} %bitcast.11, ...), custom_call_target="tpu_custom_call" | custom-call | tf_op jit(solution)/shard_map/pallas_call | solution.py:426
  46.1 1.5 %shard_map.239 = (bf16[16,1024]{1,0:T(8,128)(2,1)}, bf16[16,512]{1,0:T(8,128)(2,1)}, bf16[16,1024]{1,0:T(8,128)(2,1)}) custom-call(bf16[16,1024]{1,0:T(8,128)(2,1)} %get-tuple-element.6.a_in, bf16[16,512]{1,0:T(8,128)(2,1)} %get-tuple-element.7.b_in, bf16[16,1024]{1,0:T(8,128)(2,1)} %get-tuple-element.8.c_in), custom_call_target="tpu_custom_call" | custom-call | tf_op jit(solution)/shard_map/pallas_call | solution.py:454

commit v4 on v3

--- a/solution.py
+++ b/solution.py
@@ -69,29 +69,47 @@
     tok_hbm, len_hbm, gain_hbm, fgain_hbm, mix_hbm, routes_hbm, scores_hbm,
     wq_hbm, wk_hbm, wv_hbm, wo_hbm, ck_hbm, cv_hbm, st_hbm,
     eg_hbm, eu_hbm, ed_hbm, sg_hbm, su_hbm, sd_hbm, dg_hbm, du_hbm, dd_hbm,
-    out_ref, keys_ref, vals_ref,
+    out_ref, keys_hbm, vals_hbm,
     tok_v, len_v, gain_v, fgain_v, mix_v, routes_v, scores_v,
     wq, wk, wv, wo, ck, cv, st,
     eg, eu, ed, sg, su, sd,
-    xg, xown, wg, wt, dw, dense_v, sbuf, rbuf, ybuf, bbuf, pbuf, qbuf, qrows, decay_v, acc_v,
+    xg, xown, wg, wown, keys_v, vals_v, dw, dense_v, sbuf, rbuf, ybuf, bbuf, pbuf, qbuf, qrows, decay_v, acc_v,
     loc, lw, w_s, w_r, d_s, d_r, x_s, x_r, a_s, a_r, b_s, b_r, p_s, p_r,
 ):
     me = lax.axis_index("ep")
-    q = lax.rem(me, 8)
-    p = lax.div(me, 8)
-    z = lax.div(p, 4)
-    y = lax.rem(p, 4)
-    base = me - q
-    other = q + 1 - 2 * lax.rem(q, 2)
+    core = lax.rem(me, 2)
+    x = lax.rem(lax.div(me, 2), 4)
+    y = lax.rem(lax.div(me, 8), 4)
+    z = lax.div(me, 32)
+    xp, yp = lax.div(x, 2), lax.div(y, 2)
+    xq, yq = x + xp * (3 - 2 * x), y + yp * (3 - 2 * y)
+    q = yq * 4 + xq * 2 + core
+    t = yp * 2 + xp
+    p = z * 4 + t
+
+    def at(zz, tt, qq):
+        x_half, y_half = lax.rem(tt, 2), lax.div(tt, 2)
+        x_in, y_in = lax.rem(lax.div(qq, 2), 2), lax.div(qq, 4)
+        x_at = x_in + x_half * (3 - 2 * x_in)
+        y_at = y_in + y_half * (3 - 2 * y_in)
+        return zz * 32 + y_at * 8 + x_at * 2 + lax.rem(qq, 2)
+
+    def near(qq):
+        return at(z, t, qq)
+
+    other = q + 1 - 2 * core
 
     def mate(k):
         return lax.rem(q + k, 8)
 
-    def plane(dz, dy):
-        return lax.rem(z + dz, 4), lax.rem(y + dy, 4)
-
-    def device(zz, yy):
-        return (zz * 4 + yy) * 8 + q
+    def plane(dz, dt):
+        return lax.rem(z + dz, 4), lax.rem(t + dt, 4)
+
+    def experts_of(which):
+        return pl.ds(pl.multiple_of(which * 8, 8), 8)
+
+    def device(zz, tt):
+        return at(zz, tt, q)
 
     def remote(src, dst, s, r, dev):
         return pltpu.make_async_remote_copy(
@@ -100,30 +118,46 @@
 
     barrier = pltpu.get_barrier_semaphore()
     for k in range(1, 8):
-        pl.semaphore_signal(barrier, inc=1, device_id=(base + mate(k),), device_id_type=MESH)
-    offsets = [(dz, dy) for dz in (0, 1, 3, 2) for dy in (0, 1, 3, 2) if (dz, dy) != (0, 0)]
+        pl.semaphore_signal(barrier, inc=1, device_id=(near(mate(k)),), device_id_type=MESH)
+    offsets = [(dz, dy) for dz in (2, 0, 1, 3) for dy in (0, 1, 2, 3) if (dz, dy) != (0, 0)]
     for dz, dy in offsets:
         pl.semaphore_signal(barrier, inc=1, device_id=(device(*plane(dz, dy)),), device_id_type=MESH)
 
     own = []
     for i, hbm in enumerate((dg_hbm, du_hbm, dd_hbm)):
-        own.append(pltpu.make_async_copy(hbm, dw.at[i, q], loc.at[i]))
+        own.append(pltpu.make_async_copy(hbm, dw.at[i, q], loc.at[0]))
+    results = (
+        pltpu.make_async_copy(keys_v, keys_hbm, loc.at[1]),
+        pltpu.make_async_copy(vals_v, vals_hbm, loc.at[2]),
+    )
     fetch = {}
 
-    def want(name, hbm, ref):
-        fetch[name] = pltpu.make_async_copy(hbm, ref, lw.at[len(fetch)])
+    sems = []
+
+    def want(name, hbm, ref, group=None):
+        if group is None or group not in sems:
+            sems.append(group)
+        slot = len(sems) - 1 if group is None else sems.index(group)
+        fetch[name] = pltpu.make_async_copy(hbm, ref, lw.at[slot])
 
     def ready(*names):
         for name in names:
             fetch[name].wait()
+
+    def ready_all(group, ref):
+        pltpu.make_async_copy(ref, ref, lw.at[sems.index(group)]).wait()
+
+    def begin(*names):
+        for name in names:
+            fetch[name].start()
 
     want("tok", tok_hbm, tok_v)
     want("gain", gain_hbm, gain_v)
     want("len", len_hbm, len_v)
     want("routes", routes_hbm, routes_v)
     want("scores", scores_hbm, scores_v)
-    want("wq", wq_hbm, wq)
-    want("wk", wk_hbm, wk)
+    want("wq", wq_hbm, wq, "qk")
+    want("wk", wk_hbm, wk, "qk")
     want("wv", wv_hbm, wv)
     want("ck", ck_hbm, ck)
     for i in range(2):
@@ -132,39 +166,53 @@
         want(f"st{i}", st_hbm.at[pl.ds(4 * i, 4)], st.at[pl.ds(4 * i, 4)])
     want("wo", wo_hbm, wo)
     want("fgain", fgain_hbm, fgain_v)
-    want("sg", sg_hbm, sg)
-    want("su", su_hbm, su)
-    want("sd", sd_hbm, sd)
-    want("eg", eg_hbm.at[0], eg)
-    want("eu", eu_hbm.at[0], eu)
-    want("ed", ed_hbm.at[0], ed)
+    want("sg", sg_hbm, sg, "shared")
+    want("su", su_hbm, su, "shared")
+    want("sd", sd_hbm, sd, "shared")
+    want("eg", eg_hbm.at[0], eg, "expert")
+    want("eu", eu_hbm.at[0], eu, "expert")
+    want("ed", ed_hbm.at[0], ed, "expert")
     want("mix", mix_hbm, mix_v)
     for c in own:
         c.start()
-    for name in fetch:
-        fetch[name].start()
-
-    def shard(i, which, to):
-        block = dw.at[:, which]
-        return remote(block, block, d_s.at[i], d_r.at[i], base + to)
-
-    along = [mate(2 * k) for k in range(1, 4)]
-    first = [shard(k, q, along[k]) for k in range(3)]
-    across = [shard(3, q, other)]
-    second = [shard(4 + k, along[k], other) for k in range(3)]
+    begin("tok", "gain", "len", "routes", "scores", "wq", "wk", "wv")
+
+    up, down = q + 2 - 4 * xq, mate(4)
+    far = lax.rem(up + 4, 8)
+
+    def shard(group, which, to, cols=slice(None)):
+        block = dw.at[:, which, :, cols]
+        return remote(block, block, d_s.at[0], d_r.at[group], near(to))
+
+    def arrived(ref, sem):
+        remote(ref, ref, d_s.at[0], sem, near(other)).wait_recv()
+
+    def gone(ref, sem):
+        remote(ref, ref, sem, d_r.at[0], near(other)).wait_send()
+
+    first = [shard(0, q, up), shard(0, q, down)]
+    second = [shard(1, up, down, pl.ds(0, 512)), shard(1, down, up, pl.ds(512, 512))]
+    across = shard(2, q, other)
+    handed = [shard(2, down, other), shard(2, up, other)]
+    third = shard(2, far, other)
 
     with scope("route"):
         ready("routes", "scores")
         scores = scores_v[...]
         weight = scores / jnp.sum(scores, axis=0, keepdims=True) * route_scale
-        chosen = routes_v[...]
+        names = routes_v[...]
+        halves = ((names >> 4) & 1) * 2 + ((names >> 2) & 1)
+        x_in = ((names >> 1) & 1) ^ ((names >> 2) & 1)
+        y_in = ((names >> 3) & 1) ^ ((names >> 4) & 1)
+        chosen = (names >> 5) * 32 + halves * 8 + y_in * 4 + x_in * 2 + (names & 1)
         names = iota((128, 16), 0)
         spread = jnp.zeros((128, 16), F32)
         for k in range(6):
             spread = jnp.where(chosen[k : k + 1, :] == names, weight[k : k + 1, :], spread)
-        spread = jnp.concatenate([spread, jnp.zeros((128, 112), F32)], axis=1).T
-        wg[z, y] = spread[:16]
-
+        wown[...] = jnp.concatenate([spread, jnp.zeros((128, 112), F32)], axis=1)
+        wg[z, t] = wown[experts_of(p), :]
+
+    begin("ck", "cv0", "cv1")
     with scope("qkv"):
         ready("tok", "gain", "len")
         tok = tok_v[...].astype(F32)
@@ -177,7 +225,7 @@
         inverse = jnp.exp((lane % 64).astype(F32) * (-math.log(rope_base) / 64.0))
         sine, cosine = sin_cos(len_c * inverse)
         sine = jnp.where(lane < 64, -sine, sine)
-        ready("wq", "wk")
+        ready_all("qk", ck)
         raw_q = dot(xn, wq[...])
         raw_k = dot(xn, wk[...])
 
@@ -190,11 +238,14 @@
 
         queries = (rotate(raw_q) * 128.0 ** (-0.5)).astype(BF)
         new_keys = rotate(raw_k).astype(BF)
-        keys_ref[...] = new_keys
+        keys_v[...] = new_keys
+        results[0].start()
         ready("wv")
         new_values = dot(xn, wv[...]).astype(BF)
-        vals_ref[...] = new_values
-
+        vals_v[...] = new_values
+        results[1].start()
+
+    begin("st0", "st1", "st2", "st3", "wo", "fgain")
     with scope("rows"):
         spread_rows = onehot(iota((128, 16), 0) // 8 == iota((128, 16), 1))
         head_512 = iota((128, 512), 0) % 8 == iota((128, 512), 1) // 128
@@ -223,6 +274,7 @@
             got = dot_t(qrows[r].astype(BF), ck[2 * i : 2 * i + 2].reshape(256, 512))
             weights.append((got * decay_v[r]).astype(BF))
 
+    begin("sg", "su", "sd", "eg", "eu", "ed", "mix")
     with scope("values"):
         for i in range(8):
             if i % 4 == 0:
@@ -230,6 +282,18 @@
             r = slice(16 * i, 16 * i + 16)
             got = dot(weights[i], cv[2 * i : 2 * i + 2].reshape(256, 1024))
             acc_v[r] = acc_v[r] + by_head(got, 16)
+
+    with scope("barrier"):
+        pl.semaphore_wait(barrier, 22)
+    with scope("early"):
+        for dz, dy in offsets:
+            zz, tt = plane(dz, dy)
+            mine = wown.at[experts_of(zz * 4 + tt), :]
+            remote(mine, wg.at[z, t], w_s.at[0], w_r.at[dz], device(zz, tt)).start()
+        pltpu.make_async_copy(dw.at[:, q], dw.at[:, q], loc.at[0]).wait()
+        for c in first:
+            c.start()
+        across.start()
 
     with scope("state"):
         low = iota((16, 512), 0) < 8
@@ -244,20 +308,6 @@
             got = dot(both, st[2 * i : 2 * i + 2].reshape(1024, 256).astype(BF))
             acc_v[r] = acc_v[r] + got * carry[r]
 
-    with scope("barrier"):
-        pl.semaphore_wait(barrier, 22)
-        w_copies = {}
-        for dz, dy in offsets:
-            i = dz * 4 + dy
-            w_copies[i] = remote(
-                wg.at[z, y], wg.at[z, y], w_s.at[i], w_r.at[i], device(*plane(dz, dy))
-            )
-            w_copies[i].start()
-        for c in own:
-            c.wait()
-        for c in first + across:
-            c.start()
-
     with scope("out"):
         headed = normed(acc_v[...]).astype(BF)
         ready("wo")
@@ -269,38 +319,42 @@
         ready("fgain")
         xv = (normed(residual) * fgain_v[...]).astype(BF)
         xown[...] = xv
-        xg[z, y] = xv
-        x_copies = {}
+        xg[z, t] = xv
         for dz, dy in offsets:
-            i = dz * 4 + dy
-            x_copies[i] = remote(xown, xg.at[z, y], x_s.at[i], x_r.at[i], device(*plane(dz, dy)))
-            x_copies[i].start()
+            dev = device(*plane(dz, dy))
+            remote(xown, xg.at[z, t], x_s.at[0], x_r.at[dz], dev).start()
 
     with scope("shared"):
-        ready("sg", "su", "sd")
+        ready_all("shared", dw)
         hidden = (silu(dot(xv, sg[...])) * dot(xv, su[...])).astype(BF)
         shared = dot(hidden, sd[...])
 
-    order = (0, 1, 3, 2)
+    with scope("pump1"):
+        arrived(dw.at[:, pl.ds(0, 2)], d_r.at[0])
+        for c in second + handed:
+            c.start()
+
     before = onehot(
         (iota((128, 128), 0) < iota((128, 128), 1))
         & (iota((128, 128), 0) // 16 == iota((128, 128), 1) // 16)
     )
     slot = iota((8, 8, 128), 1)
     sender = iota((8, 8, 128), 2) // 16
-    out_copies, picks, rows_of = {}, {}, {}
-    for dz in order:
-        zz = lax.rem(z + 4 - dz, 4)
-        rows_of[dz] = zz
+    picks = {}
+
+    def row_at(dz):
+        return lax.rem(z + 4 - dz, 4)
+
+    def dispatch(dz):
+        zz = row_at(dz)
         with scope(f"xwait{dz}"):
-            for dy in range(4):
-                if (dz, dy) != (0, 0):
-                    w_copies[dz * 4 + dy].wait_recv()
-                    x_copies[dz * 4 + dy].wait_recv()
+            count = pl.ds(0, 3 if dz == 0 else 4)
+            arrived(wg.at[zz, count], w_r.at[dz])
+            arrived(xg.at[zz, count], x_r.at[dz])
         with scope(f"send{dz}"):
-            w_all = jnp.concatenate([wg[zz].reshape(64, 128), jnp.zeros((64, 128), F32)], axis=0)
-            wt[dz] = w_all.T
-            w_p = wt[dz, pl.ds(pl.multiple_of(p * 8, 8), 8), :]
+            w_p = wg[zz, 0]
+            for d in range(1, 4):
+                w_p = w_p + pltpu.roll(wg[zz, d], 16 * d, 1)
             r_p = dot(onehot(w_p > 0), before)
             w_b = jnp.broadcast_to(w_p[:, None, :], (8, 8, 128))
             r_b = jnp.broadcast_to(r_p[:, None, :], (8, 8, 128))
@@ -310,56 +364,27 @@
             choose = onehot(picked > 0)[:, :64]
             sbuf[zz] = dot(choose, xg[zz].reshape(64, 1024)).astype(BF).reshape(8, 8, 1024)
             for k in range(1, 8):
-                i = dz * 8 + k
-                out_copies[i] = remote(
-                    sbuf.at[zz, mate(k)], rbuf.at[zz, q], a_s.at[i], a_r.at[i], base + mate(k)
-                )
-                out_copies[i].start()
+                to = mate(k)
+                remote(sbuf.at[zz, to], rbuf.at[zz, q], a_s.at[0], a_r.at[dz], near(to)).start()
             rbuf[zz, q] = sbuf[zz, q]
 
-    with scope("dfwd"):
-        for k in range(3):
-            first[k].wait_recv()
-            second[2 - k].start()
-
-    ready("eg", "eu", "ed")
-    back_copies = {}
-    for dz in order:
-        zz = rows_of[dz]
+    def expert(dz):
+        zz = row_at(dz)
         with scope(f"ewait{dz}"):
-            for k in range(1, 8):
-                out_copies[dz * 8 + k].wait_recv()
+            arrived(rbuf.at[zz, pl.ds(0, 7)], a_r.at[dz])
         with scope(f"expert{dz}"):
             rows = rbuf[zz].reshape(64, 1024)
             hid = (silu(dot(rows, eg[...])) * dot(rows, eu[...])).astype(BF)
             ybuf[zz] = dot(hid, ed[...]).astype(BF).reshape(8, 8, 1024)
             for k in range(1, 8):
-                i = dz * 8 + k
-                back_copies[i] = remote(
-                    ybuf.at[zz, mate(k)], bbuf.at[zz, q], b_s.at[i], b_r.at[i], base + mate(k)
-                )
-                back_copies[i].start()
+                to = mate(k)
+                remote(ybuf.at[zz, to], bbuf.at[zz, q], b_s.at[0], b_r.at[dz], near(to)).start()
             bbuf[zz, q] = ybuf[zz, q]
 
-    with scope("dwait"):
-        for c in across + second:
-            c.wait_recv()
-
-    with scope("dense"):
-        tokens = xg[...].reshape(256, 1024)
-        gate = dot_t(tokens, dw[0].reshape(256, 1024))
-        up = dot_t(tokens, dw[1].reshape(256, 1024))
-        ready("mix")
-        mix = 1.0 / (1.0 + jnp.exp(-mix_v[...]))
-        down = dw[2].reshape(256, 1024)
-        dense_v[...] = (dot((silu(gate) * up).astype(BF), down) * mix).reshape(4, 64, 1024)
-
-    p_copies = {}
-    for dz in order:
-        zz = rows_of[dz]
+    def gather(dz):
+        zz = row_at(dz)
         with scope(f"bwait{dz}"):
-            for k in range(1, 8):
-                back_copies[dz * 8 + k].wait_recv()
+            arrived(bbuf.at[zz, pl.ds(0, 7)], b_r.at[dz])
         with scope(f"combine{dz}"):
             combine = picks[dz].T[:64]
             comb_hi = combine.astype(BF)
@@ -367,28 +392,54 @@
             back = bbuf[zz].reshape(64, 1024)
             partial = dense_v[zz] + dot(comb_hi, back) + dot(comb_lo, back)
             pbuf[zz] = partial.astype(BF).reshape(4, 16, 1024)
-            for dy in (0, 1, 3, 2):
+            for dy in (2, 1, 3, 0):
                 if (dz, dy) != (0, 0):
-                    yy = lax.rem(y + 4 - dy, 4)
-                    i = dz * 4 + dy
-                    p_copies[i] = remote(
-                        pbuf.at[zz, yy], qbuf.at[z, y], p_s.at[i], p_r.at[i], device(zz, yy)
-                    )
-                    p_copies[i].start()
-    qbuf[z, y] = pbuf[z, y]
+                    tt = lax.rem(t + 4 - dy, 4)
+                    sums = pbuf.at[zz, tt]
+                    remote(sums, qbuf.at[p], p_s.at[0], p_r.at[0], device(zz, tt)).start()
+
+    dispatch(0)
+    dispatch(2)
+    dispatch(1)
+    ready_all("expert", dw)
+    expert(0)
+    dispatch(3)
+    with scope("pump2"):
+        arrived(dw.at[:, 0], d_r.at[1])
+        third.start()
+    expert(2)
+    with scope("dwait"):
+        arrived(dw.at[:, pl.ds(0, 4)], d_r.at[2])
+    with scope("dense"):
+        tokens = xg[...].reshape(256, 1024)
+        gate = dot_t(tokens, dw[0].reshape(256, 1024))
+        raised = dot_t(tokens, dw[1].reshape(256, 1024))
+        ready("mix")
+        mix = 1.0 / (1.0 + jnp.exp(-mix_v[...]))
+        lowered = dot((silu(gate) * raised).astype(BF), dw[2].reshape(256, 1024))
+        dense_v[...] = (lowered * mix).reshape(4, 64, 1024)
+    expert(1)
+    expert(3)
+    gather(0)
+    gather(2)
+    gather(1)
+    gather(3)
+    qbuf[p] = pbuf[z, t]
     with scope("pwait"):
-        for i in p_copies:
-            p_copies[i].wait_recv()
+        arrived(qbuf.at[pl.ds(0, 15)], p_r.at[0])
     with scope("final"):
-        total = shared + jnp.sum(qbuf[...].reshape(16, 16, 1024).astype(F32), axis=0)
+        total = shared + jnp.sum(qbuf[...].astype(F32), axis=0)
         out_ref[...] = (residual + normed(total)).astype(BF)
 
     with scope("drain"):
-        for c in first + across + second:
-            c.wait_send()
-        for group in (w_copies, x_copies, out_copies, back_copies, p_copies):
-            for i in group:
-                group[i].wait_send()
+        for c in results:
+            c.wait()
+        gone(dw.at[:, pl.ds(0, 7)], d_s.at[0])
+        gone(wown.at[pl.ds(0, 120), :], w_s.at[0])
+        gone(qbuf.at[pl.ds(0, 15)], x_s.at[0])
+        gone(sbuf.at[:, pl.ds(0, 7)], a_s.at[0])
+        gone(ybuf.at[:, pl.ds(0, 7)], b_s.at[0])
+        gone(qbuf.at[pl.ds(0, 15)], p_s.at[0])
 
 
 def results_kernel(a_in, b_in, c_in, a_out, b_out, c_out, a_v, b_v, c_v, in_s, out_s):
@@ -427,13 +478,15 @@
         layer_kernel,
         out_shape=shapes,
         in_specs=[hbm] * len(args),
-        out_specs=(vm, vm, vm),
+        out_specs=(vm, hbm, hbm),
         scratch_shapes=[pltpu.VMEM(s, a.dtype) for s, a in zip(local, args)]
         + [
             pltpu.VMEM((4, 4, 16, 1024), BF),
             pltpu.VMEM((16, 1024), BF),
-            pltpu.VMEM((4, 4, 16, 128), F32),
-            pltpu.VMEM((4, 128, 128), F32),
+            pltpu.VMEM((4, 4, 8, 128), F32),
+            pltpu.VMEM((128, 128), F32),
+            pltpu.VMEM((16, 512), BF),
+            pltpu.VMEM((16, 1024), BF),
             pltpu.VMEM((3, 8, 32, 1024), BF),
             pltpu.VMEM((4, 64, 1024), F32),
             pltpu.VMEM((4, 8, 8, 1024), BF),
@@ -441,13 +494,13 @@
             pltpu.VMEM((4, 8, 8, 1024), BF),
             pltpu.VMEM((4, 8, 8, 1024), BF),
             pltpu.VMEM((4, 4, 16, 1024), BF),
-            pltpu.VMEM((4, 4, 16, 1024), BF),
+            pltpu.VMEM((16, 16, 1024), BF),
             pltpu.VMEM((128, 512), F32),
             pltpu.VMEM((128, 256), F32),
             pltpu.VMEM((128, 256), F32),
-            dma((3,)), dma((24,)), dma((16,)), dma((16,)), dma((8,)), dma((8,)),
-            dma((16,)), dma((16,)), dma((32,)), dma((32,)), dma((32,)), dma((32,)),
-            dma((16,)), dma((16,)),
+            dma((3,)), dma((19,)), dma((1,)), dma((4,)), dma((1,)), dma((3,)),
+            dma((1,)), dma((4,)), dma((1,)), dma((4,)), dma((1,)), dma((4,)),
+            dma((1,)), dma((1,)),
         ],
         compiler_params=pltpu.CompilerParams(collective_id=0, has_side_effects=True),
     )(*args)

time: 47.7 us -> 43.4 us (0.910)
  Pallas kernels: 46.9 us -> 42.6 us
    pallas_call x1, Pallas kernels: 45.4 us -> 41.2 us  [per_device(): pl.pallas_call(layer_kernel, out_shape=shapes, in_specs=[hbm] * len(args)...]
where the time goes in v4:
time: 43.4 us; the launch traced here: 43.3 us
  Pallas kernels  42.6 us (98%)
  between operations  0.65 us (1%)
    pallas_call x1, Pallas kernels, per_device(): pl.pallas_call(layer_kernel, out_shape=shapes, in_specs=[hbm] * len(args)...  41.2 us
    pallas_call x1, Pallas kernels, per_device(): pl.pallas_call(results_kernel, out_shape=shapes, in_specs=[hbm] * 3, out_...  1.46 us

profile of v4, /device:TPU:1, one launch (start us, length us, event | category | flops | bytes accessed | tf_op | source)
XLA Modules:
  0.0 43.3 jit_solution(4229665229339587239)
XLA Ops:
  0.6 41.2 %shard_map.238 = (bf16[16,1024]{1,0:T(8,128)(2,1)}, bf16[16,512]{1,0:T(8,128)(2,1)}, bf16[16,1024]{1,0:T(8,128)(2,1)}) custom-call(bf16[16,1024]{1,0:T(8,128)(2,1)} %tok_hbm.1, s32[1,16]{1,0:T(1,128)} %bitcast.13, f32[1,1024]{1,0:T(1,128)} %bitcast.8, f32[1,1024]{1,0:T(1,128)} %bitcast.9, f32[1,1024]{1,0:T(1,128)} %bitcast.10, s32[6,16]{1,0:T(8,128)} %bitcast.11, ...), custom_call_target="tpu_custom_call" | custom-call | tf_op jit(solution)/shard_map/pallas_call | solution.py:477
  41.8 1.5 %shard_map.239 = (bf16[16,1024]{1,0:T(8,128)(2,1)}, bf16[16,512]{1,0:T(8,128)(2,1)}, bf16[16,1024]{1,0:T(8,128)(2,1)}) custom-call(bf16[16,1024]{1,0:T(8,128)(2,1)} %get-tuple-element.6.a_in, bf16[16,512]{1,0:T(8,128)(2,1)} %get-tuple-element.7.b_in, bf16[16,1024]{1,0:T(8,128)(2,1)} %get-tuple-element.8.c_in), custom_call_target="tpu_custom_call" | custom-call | tf_op jit(solution)/shard_map/pallas_call | solution.py:507

commit v5 on v4

--- a/solution.py
+++ b/solution.py
@@ -180,6 +180,9 @@
     up, down = q + 2 - 4 * xq, mate(4)
     far = lax.rem(up + 4, 8)
 
+    turn = 1 - 2 * core
+    reach = (up + turn, down + turn, far + turn, far, down, up, other)
+
     def shard(group, which, to, cols=slice(None)):
         block = dw.at[:, which, :, cols]
         return remote(block, block, d_s.at[0], d_r.at[group], near(to))
@@ -266,23 +269,6 @@
         carry = jnp.exp((fill + 1.0) * rate)
         acc_v[...] = own_w * by_head(dot(spread_rows, new_values), 128)
 
-    with scope("scores"):
-        ready("ck")
-        weights = []
-        for i in range(8):
-            r = slice(16 * i, 16 * i + 16)
-            got = dot_t(qrows[r].astype(BF), ck[2 * i : 2 * i + 2].reshape(256, 512))
-            weights.append((got * decay_v[r]).astype(BF))
-
-    begin("sg", "su", "sd", "eg", "eu", "ed", "mix")
-    with scope("values"):
-        for i in range(8):
-            if i % 4 == 0:
-                ready(f"cv{i // 4}")
-            r = slice(16 * i, 16 * i + 16)
-            got = dot(weights[i], cv[2 * i : 2 * i + 2].reshape(256, 1024))
-            acc_v[r] = acc_v[r] + by_head(got, 16)
-
     with scope("barrier"):
         pl.semaphore_wait(barrier, 22)
     with scope("early"):
@@ -294,6 +280,23 @@
         for c in first:
             c.start()
         across.start()
+
+    with scope("scores"):
+        ready("ck")
+        weights = []
+        for i in range(8):
+            r = slice(16 * i, 16 * i + 16)
+            got = dot_t(qrows[r].astype(BF), ck[2 * i : 2 * i + 2].reshape(256, 512))
+            weights.append((got * decay_v[r]).astype(BF))
+
+    begin("sg", "su", "sd", "eg", "eu", "ed", "mix")
+    with scope("values"):
+        for i in range(8):
+            if i % 4 == 0:
+                ready(f"cv{i // 4}")
+            r = slice(16 * i, 16 * i + 16)
+            got = dot(weights[i], cv[2 * i : 2 * i + 2].reshape(256, 1024))
+            acc_v[r] = acc_v[r] + by_head(got, 16)
 
     with scope("state"):
         low = iota((16, 512), 0) < 8
@@ -363,8 +366,7 @@
             picks[dz] = picked
             choose = onehot(picked > 0)[:, :64]
             sbuf[zz] = dot(choose, xg[zz].reshape(64, 1024)).astype(BF).reshape(8, 8, 1024)
-            for k in range(1, 8):
-                to = mate(k)
+            for to in reach:
                 remote(sbuf.at[zz, to], rbuf.at[zz, q], a_s.at[0], a_r.at[dz], near(to)).start()
             rbuf[zz, q] = sbuf[zz, q]
 
@@ -376,8 +378,7 @@
             rows = rbuf[zz].reshape(64, 1024)
             hid = (silu(dot(rows, eg[...])) * dot(rows, eu[...])).astype(BF)
             ybuf[zz] = dot(hid, ed[...]).astype(BF).reshape(8, 8, 1024)
-            for k in range(1, 8):
-                to = mate(k)
+            for to in reach:
                 remote(ybuf.at[zz, to], bbuf.at[zz, q], b_s.at[0], b_r.at[dz], near(to)).start()
             bbuf[zz, q] = ybuf[zz, q]
 

time: 43.4 us -> 43.1 us (level)
  Pallas kernels: 42.6 us -> 41.9 us
    pallas_call x1, Pallas kernels: 41.2 us -> 40.5 us  [per_device(): pl.pallas_call(layer_kernel, out_shape=shapes, in_specs=[hbm] * len(args)...]
where the time goes in v5:
time: 43.1 us; the launch traced here: 42.6 us
  Pallas kernels  41.9 us (97%)
  between operations  0.65 us (2%)
    pallas_call x1, Pallas kernels, per_device(): pl.pallas_call(layer_kernel, out_shape=shapes, in_specs=[hbm] * len(args)...  40.5 us
    pallas_call x1, Pallas kernels, per_device(): pl.pallas_call(results_kernel, out_shape=shapes, in_specs=[hbm] * 3, out_...  1.46 us

profile of v5, /device:TPU:1, one launch (start us, length us, event | category | flops | bytes accessed | tf_op | source)
XLA Modules:
  0.0 42.6 jit_solution(7602676648932118278)
XLA Ops:
  0.6 40.5 %shard_map.238 = (bf16[16,1024]{1,0:T(8,128)(2,1)}, bf16[16,512]{1,0:T(8,128)(2,1)}, bf16[16,1024]{1,0:T(8,128)(2,1)}) custom-call(bf16[16,1024]{1,0:T(8,128)(2,1)} %tok_hbm.1, s32[1,16]{1,0:T(1,128)} %bitcast.13, f32[1,1024]{1,0:T(1,128)} %bitcast.8, f32[1,1024]{1,0:T(1,128)} %bitcast.9, f32[1,1024]{1,0:T(1,128)} %bitcast.10, s32[6,16]{1,0:T(8,128)} %bitcast.11, ...), custom_call_target="tpu_custom_call" | custom-call | tf_op jit(solution)/shard_map/pallas_call | solution.py:478
  41.1 1.5 %shard_map.239 = (bf16[16,1024]{1,0:T(8,128)(2,1)}, bf16[16,512]{1,0:T(8,128)(2,1)}, bf16[16,1024]{1,0:T(8,128)(2,1)}) custom-call(bf16[16,1024]{1,0:T(8,128)(2,1)} %get-tuple-element.6.a_in, bf16[16,512]{1,0:T(8,128)(2,1)} %get-tuple-element.7.b_in, bf16[16,1024]{1,0:T(8,128)(2,1)} %get-tuple-element.8.c_in), custom_call_target="tpu_custom_call" | custom-call | tf_op jit(solution)/shard_map/pallas_call | solution.py:508
